TPU v7x, 512 devices: a whole 4x4x16 slice. The times are simulated.
512 devices in a mesh: ep: 128 (over z, x, core), tp: 4 (over y).
Axes of the slice: x: 4, y: 4, z: 16, core: 2. Of those that a mesh axis runs over, the one named last changes fastest.
Arguments:
- tokens: bfloat16 [1024, 1024], P('ep'), may hold values from -6 to 6
- kv_cache: bfloat16 [1024, 4, 1024, 128], P('ep', 'tp'), may hold values from -6 to 6
- lengths: int32 [1024], P('ep'), may hold values from 256 to 1024
- w_query: bfloat16 [1024, 512], P(None, 'tp'), may hold values from -0.1875 to 0.1875
- w_key: bfloat16 [1024, 256], P(None, 'tp'), may hold values from -0.1875 to 0.1875
- w_value: bfloat16 [1024, 256], P(None, 'tp'), may hold values from -0.1875 to 0.1875
- break_bias: float32 [8], P('tp'), may hold values from -7.5 to -3.5
- head_gain: float32 [512], P('tp'), may hold values from 0.1 to 1.9
- w_output: bfloat16 [512, 1024], P('tp'), may hold values from -0.25 to 0.25
- attn_norm_gain: float32 [1024], replicated, may hold values from 0.1 to 1.9
- w_router: bfloat16 [1024, 16], replicated, may hold values from -0.1875 to 0.1875
- routes: int32 [1024, 2], P('ep'), may hold values from 0 to 15, all different within a row; in each aligned block of 8 rows (0 to 7, 8 to 15, ...) at most 2 rows name the same one
- expert_gate: bfloat16 [1024, 57344], P(None, ('ep', 'tp')), may hold values from -0.1875 to 0.1875
- expert_up: bfloat16 [1024, 57344], P(None, ('ep', 'tp')), may hold values from -0.1875 to 0.1875
- expert_down: bfloat16 [57344, 1024], P(('ep', 'tp')), may hold values from -0.09375 to 0.09375
- dense_gate: bfloat16 [1024, 2816], P(None, 'ep'), may hold values from -0.1875 to 0.1875
- dense_up: bfloat16 [1024, 2816], P(None, 'ep'), may hold values from -0.1875 to 0.1875
- dense_down: bfloat16 [2816, 1024], P('ep', 'tp'), may hold values from -0.109375 to 0.109375
- mix_gate: bfloat16 [1024], replicated, may hold values from -0.1875 to 0.1875
- ffn_norm_gain: float32 [1024], P('tp'), may hold values from 0.1 to 1.9
Outputs:
- layer_out: bfloat16 [1024, 1024], P('ep', 'tp')
- new_kv: bfloat16 [1024, 4, 128], P('ep', 'tp')
Inputs may be any that keep to these rules, and one draw needn't show every extreme that they name: lengths[b] is the number of valid cached positions of sequence b and the new token's position. `routes`: each row names 2 different experts. Among the rows of one index of ep (aligned blocks of 8 rows) no expert is named more than 2 times, a bound that some block reaches.
All inputs are finite; a program needn't handle non-finite values.
Results may differ from a plain program's by a relative error of at most 0.012.
Values may be sent and summed in bfloat16 or wider, within the bound.
A program may use at most 128 MiB of HBM per device.

v0:
```python
import jax
import jax.numpy as jnp
from jax import lax
from jax.sharding import Mesh
from jax.sharding import PartitionSpec as P

FE = 3584
CAP = 2
EP = ("ep_0", "ep_1", "ep_2")
EP_TP = ("ep_0", "ep_1", "ep_2", "tp")


RESIDUAL_SCALE = 8.0**0.25
PRECISE = lax.Precision.HIGHEST


def from_everyone(shard, axis):
    copies = jnp.broadcast_to(shard, (lax.axis_size(axis), *shard.shape))
    return lax.all_to_all(copies, axis, split_axis=0, concat_axis=0, tiled=True)


def of_everyone(shard, axis):
    everything = from_everyone(shard, axis)
    return jnp.sum(everything.astype(jnp.float32), axis=0)


def cut_along(shard, dim, peers):
    shape = shard.shape
    tiles = shard.reshape(*shape[:dim], peers, shape[dim] // peers, *shape[dim + 1 :])
    return jnp.moveaxis(tiles, dim, 0)


def summed_on_arrival(shard, axis, dim):
    peers = lax.axis_size(axis)
    tiles = lax.all_to_all(cut_along(shard, dim, peers), axis, 0, 0, tiled=True)
    return jnp.sum(tiles.astype(jnp.float32), axis=0)


def joined_along(tiles, dim):
    tiles = jnp.moveaxis(tiles, 0, dim)
    shape = tiles.shape
    return tiles.reshape(*shape[:dim], shape[dim] * shape[dim + 1], *shape[dim + 2 :])


def stacked_from(shard, axes, sequence):
    tiles = shard[None]
    for k in sequence:
        tiles = lax.all_gather(tiles, axes[k], axis=0, tiled=True)
    block = [lax.axis_size(axes[k]) for k in reversed(sequence)]
    tiles = tiles.reshape(*block, *shard.shape)
    turned = sorted(range(len(sequence)), key=lambda place: sequence[len(sequence) - 1 - place])
    return tiles.transpose(*turned, *range(len(sequence), tiles.ndim)).reshape(-1, *shard.shape)


def gathered_by_axis(shard, axes, sequence, dim):
    return joined_along(stacked_from(shard, axes, sequence), dim)


def of_everyone_2(shard, axis):
    return from_everyone(shard, axis).sum(axis=0)


def together(arrays, axis):
    ends = [0]
    for a in arrays:
        ends.append(ends[-1] + a.size)
    so_far = of_everyone_2(jnp.concatenate([a.ravel() for a in arrays]), axis)
    return tuple((so_far[b:e].reshape(a.shape) for a, b, e in zip(arrays, ends, ends[1:])))


def layer_norm(values, gain):
    centre = jnp.mean(values, axis=-1, keepdims=True)
    centred = values - centre
    spread = jnp.mean(centred * centred, axis=-1, keepdims=True)
    return centred * lax.rsqrt(spread + 1e-05) * gain


def stick_weights(scores, visible):
    survive = jnp.where(visible, jax.nn.log_sigmoid(-scores), 0.0)
    remaining = lax.cumsum(survive, axis=3, reverse=True) - survive
    return jnp.where(visible, jnp.exp(jax.nn.log_sigmoid(scores) + remaining), 0.0)


def body(
    tokens,
    kv_cache,
    lengths,
    w_query,
    w_key,
    w_value,
    break_bias,
    head_gain,
    w_output,
    attn_norm_gain,
    w_router,
    routes,
    expert_gate,
    expert_up,
    expert_down,
    dense_gate,
    dense_up,
    dense_down,
    mix_gate,
    ffn_norm_gain,
):
    seq_count = tokens.shape[0]
    model_width = tokens.shape[1]
    key_heads = kv_cache.shape[1]
    positions = kv_cache.shape[2]
    head_dim = kv_cache.shape[3] // 2
    local_heads = w_query.shape[1] // head_dim
    group_size = local_heads // key_heads
    queries = jnp.dot(tokens, w_query, preferred_element_type=jnp.float32).astype(jnp.bfloat16)
    queries = queries.reshape(seq_count, key_heads, group_size, head_dim)
    key_new = jnp.dot(tokens, w_key, preferred_element_type=jnp.float32).astype(jnp.bfloat16)
    value_new = jnp.dot(tokens, w_value, preferred_element_type=jnp.float32).astype(jnp.bfloat16)
    new_kv = jnp.concatenate(
        [
            key_new.reshape(seq_count, key_heads, head_dim),
            value_new.reshape(seq_count, key_heads, head_dim),
        ],
        axis=2,
    )
    cached_keys = kv_cache[..., :head_dim]
    cached_values = kv_cache[..., head_dim:]
    scores = jnp.einsum(
        "bgqd,bgld->bgql", queries, cached_keys, preferred_element_type=jnp.float32
    ) * head_dim ** (-0.5)
    scores = scores + break_bias.reshape(1, key_heads, group_size, 1)
    visible = lax.broadcasted_iota(jnp.int32, (seq_count, 1, 1, positions), 3) < lengths.reshape(
        seq_count, 1, 1, 1
    )
    weights = stick_weights(scores, visible).astype(jnp.bfloat16)
    blended = jnp.einsum(
        "bgql,bgld->bgqd", weights, cached_values, preferred_element_type=jnp.float32
    )
    rescale = lax.rsqrt(jnp.mean(blended * blended, axis=3, keepdims=True) + 1e-06)
    normed = ((blended * rescale).reshape(seq_count, local_heads * head_dim) * head_gain).astype(
        jnp.bfloat16
    )
    partial_out = jnp.dot(normed, w_output, preferred_element_type=jnp.float32)
    attended = of_everyone(partial_out.astype(jnp.bfloat16), "tp").astype(jnp.float32)
    settled = layer_norm(
        RESIDUAL_SCALE * tokens.astype(jnp.float32) + attended, attn_norm_gain
    ).astype(jnp.bfloat16)
    experts = w_router.shape[1]
    top_count = routes.shape[1]
    logits = jnp.dot(settled, w_router, preferred_element_type=jnp.float32)
    chosen = routes[:, :, None] == lax.broadcasted_iota(
        jnp.int32, (seq_count, top_count, experts), 2
    )
    picked = jnp.sum(jnp.where(chosen, logits[:, None, :], 0.0), axis=2)
    route_weight = jax.nn.sigmoid(picked - picked[:, ::-1])
    assigned = chosen.reshape(seq_count * top_count, experts).astype(jnp.int32)
    before = jnp.cumsum(assigned, axis=0) - assigned
    slot_index = jnp.sum(before * assigned, axis=1)
    slot_hits = (
        slot_index[:, None] == lax.broadcasted_iota(jnp.int32, (seq_count * top_count, CAP), 1)
    ).astype(jnp.int32)
    placement = (assigned[:, :, None] * slot_hits[:, None, :]).reshape(
        seq_count, top_count, experts * CAP
    )
    selector = jnp.sum(placement, axis=1).astype(jnp.bfloat16)
    weighted = jnp.sum(placement.astype(jnp.float32) * route_weight[:, :, None], axis=1)
    buffer = lax.dot_general(
        selector, settled, (((0,), (0,)), ((), ())), preferred_element_type=jnp.float32
    )
    buffer = buffer.astype(jnp.bfloat16).reshape(experts, CAP, model_width)
    hosts = lax.axis_size(EP)
    tp_size = lax.axis_size("tp")
    per_host = 1
    outgoing = jnp.repeat(buffer, hosts // experts, axis=0).reshape(hosts, 1, CAP, model_width)
    columns = expert_gate.shape[1]
    block_index = lax.axis_index(EP_TP)
    own_expert = block_index * columns // FE
    local_slot = own_expert - lax.axis_index(EP) * experts // hosts
    slice_width = model_width // tp_size
    arrived = lax.all_to_all(outgoing, EP, split_axis=0, concat_axis=0, tiled=True)
    slot_count = arrived.shape[2]
    received = lax.dynamic_index_in_dim(arrived, local_slot, 1, keepdims=False)
    received = received.reshape(hosts * slot_count, model_width)
    gate_pre = jnp.dot(received, expert_gate, preferred_element_type=jnp.float32)
    up_pre = jnp.dot(received, expert_up, preferred_element_type=jnp.float32)
    hidden = (jax.nn.silu(gate_pre) * up_pre).astype(jnp.bfloat16)
    partial_value = jnp.dot(hidden, expert_down, preferred_element_type=jnp.float32)
    partial_value = partial_value.reshape(hosts, 1, slot_count, model_width)
    slot_mask = (lax.broadcasted_iota(jnp.int32, (1, per_host, 1, 1), 1) == local_slot).astype(
        jnp.float32
    )
    summed = summed_on_arrival((partial_value * slot_mask).astype(jnp.bfloat16), "tp", 3)
    returned = lax.all_to_all(
        summed.astype(jnp.bfloat16), EP, split_axis=0, concat_axis=0, tiled=True
    ).astype(summed.dtype)
    host_ids = lax.broadcasted_iota(jnp.int32, (hosts * per_host,), 0)
    host_expert = host_ids // per_host * experts // hosts + host_ids % per_host
    ownership = (
        host_expert[None, :] == lax.broadcasted_iota(jnp.int32, (experts, hosts * per_host), 0)
    ).astype(jnp.float32)
    gathered = jnp.dot(
        ownership, returned.reshape(hosts * per_host, CAP * slice_width), precision=PRECISE
    )
    gathered = gathered.reshape(experts * CAP, slice_width)
    routed = jnp.dot(weighted, gathered, precision=PRECISE)
    column_rank = lax.axis_index("tp")
    own_settled = lax.dynamic_slice_in_dim(settled, column_rank * slice_width, slice_width, 1)
    shard_rows = lax.all_gather(settled, EP, axis=0, tiled=True)
    gate_pre = jnp.dot(shard_rows, dense_gate, preferred_element_type=jnp.float32)
    up_pre = jnp.dot(shard_rows, dense_up, preferred_element_type=jnp.float32)
    dense_hidden = (jax.nn.silu(gate_pre) * up_pre).astype(jnp.bfloat16)
    own_hidden = lax.all_to_all(dense_hidden, EP, split_axis=0, concat_axis=1, tiled=True)
    dense_out = jnp.dot(
        own_hidden,
        gathered_by_axis(dense_down, EP, (0, 1, 2), 0),
        preferred_element_type=jnp.float32,
    )
    mix_weight = jax.nn.sigmoid(jnp.dot(settled, mix_gate, preferred_element_type=jnp.float32))
    combined = (
        RESIDUAL_SCALE * own_settled.astype(jnp.float32) + routed + mix_weight[:, None] * dense_out
    )
    row_sums, squares = together(
        (jnp.sum(combined, axis=1), jnp.sum(combined * combined, axis=1)), "tp"
    )
    row_mean = row_sums / model_width
    row_var = squares / model_width - row_mean * row_mean
    result = (
        (combined - row_mean[:, None]) * lax.rsqrt(row_var[:, None] + 1e-05) * ffn_norm_gain
    ).astype(jnp.bfloat16)
    return (result, new_kv)


def solution(mesh):
    split = Mesh(mesh.devices.reshape(16, 4, 2, mesh.shape["tp"]), ("ep_0", "ep_1", "ep_2", "tp"))
    return jax.shard_map(
        body,
        mesh=split,
        in_specs=(
            P(EP, None),
            P(EP, "tp", None, None),
            P(EP),
            P(None, "tp"),
            P(None, "tp"),
            P(None, "tp"),
            P("tp"),
            P("tp"),
            P("tp", None),
            P(),
            P(),
            P(EP, None),
            P(None, EP_TP),
            P(None, EP_TP),
            P(EP_TP, None),
            P(None, EP),
            P(None, EP),
            P(EP, "tp"),
            P(),
            P("tp"),
        ),
        out_specs=(P(EP, "tp"), P(EP, "tp", None)),
        check_vma=False,
    )
```

profile of v0, /device:TPU:6, one launch (start us, length us, event | category | flops | bytes accessed | tf_op | source)
XLA Modules:
  0.0 306.7 jit_solution(8504936146442683302)
XLA Ops:
  7.2 0.9 iota_compare_fusion
  8.1 1.1 convolution_convert_fusion.4
  9.2 0.1 reshape.271
  9.3 2.3 fusion.31
  11.6 19.8 %reduce-window.6 = f32[8,1,2,8,128]{4,3,2,1,0:T(8,128)S(1)} reduce-window(f32[8,1,2,8,128]{4,3,2,1,0:T(8,128)S(1)} %bitcast.88, f32[]{:T(128)} %constant.108.clone.1), window={size=1x1x1x1x128 pad=0_0x0_0x0_0x0_0x0_127}, to_apply=%region_0.1 | reduce-window | flops 2080768 | bytes 131076 | tf_op jit(solution)/shard_map/reduce-window
  31.5 0.2 copy.65
  31.6 0.3 reduce-window.9
  32.0 0.1 broadcast.213
  32.2 1.1 multiply_reduce_fusion.3
  33.4 0.1 broadcast_multiply_fusion.1
  33.4 0.1 reshape.279
  33.5 0.2 convolution_convert_fusion.1
  33.7 0.6 broadcast_in_dim.35
  34.3 4.5 %all-to-all-start = ((bf16[4,8,1024]{2,1,0:T(8,128)(2,1)}), bf16[4,8,1024]{2,1,0:T(8,128)(2,1)S(1)}, u32[]{:S(2)}, u32[]{:S(2)}) async-start(bf16[4,8,1024]{2,1,0:T(8,128)(2,1)} %broadcast_in_dim.35), calls=%async_computation | async-start | bytes 131072 | tf_op jit(solution)/shard_map/all_to_all | solution.py:19
  38.8 36.4 %all-gather.1 = bf16[16,22,256]{2,1,0:T(8,128)(2,1)S(1)} all-gather(bf16[1,22,256]{2,1,0:T(8,128)(2,1)S(1)} %bitcast.90), channel_id=2, replica_groups=mesh['ep_0'=16,'ep_1'=4,'ep_2'=2,'tp'=4] {'ep_0'}, dimensions={0}, use_global_device_ids=true | all-gather | bytes 191488 | tf_op jit(solution)/shard_map/all_gather | solution.py:48
  75.3 14.0 %all_gather.14 = bf16[64,22,256]{2,0,1:T(8,128)(2,1)} all-gather(bf16[16,22,256]{2,0,1:T(8,128)(2,1)S(1)} %copy.73), channel_id=1, replica_groups=mesh['ep_0'=16,'ep_1'=4,'ep_2'=2,'tp'=4] {'ep_1'}, dimensions={0}, use_global_device_ids=true | all-gather | bytes 901120 | tf_op jit(solution)/shard_map/all_gather | solution.py:48
  89.4 0.1 copy.68
  89.5 0.1 eq.48
  89.7 0.2 select_reduce_fusion.1
  90.0 0.1 fusion.34
  90.1 0.2 multiply_reduce_fusion
  90.3 0.7 multiply_convert_fusion
  91.0 0.1 broadcast_multiply_fusion
  91.1 0.1 mul.204
  91.3 1.0 convolution_convert_fusion
  92.3 1.1 broadcast_in_dim.58
  93.4 10.6 %all-to-all-start.1 = ((bf16[128,1,2,1024]{3,2,1,0:T(2,128)(2,1)}), bf16[128,1,2,1024]{3,2,1,0:T(2,128)(2,1)S(1)}, u32[]{:S(2)}, u32[]{:S(2)}) async-start(bf16[128,1,2,1024]{3,2,1,0:T(2,128)(2,1)} %bitcast.5), calls=%async_computation.1 | async-start | bytes 1048576 | tf_op jit(solution)/shard_map/all_to_all | solution.py:178
  104.1 0.1 fusion.16
  104.2 0.1 fusion.17
  104.4 32.3 %all-to-all-done.1 = bf16[128,1,2,1024]{3,2,1,0:T(2,128)(2,1)S(1)} async-done(((bf16[128,1,2,1024]{3,2,1,0:T(2,128)(2,1)}), bf16[128,1,2,1024]{3,2,1,0:T(2,128)(2,1)S(1)}, u32[]{:S(2)}, u32[]{:S(2)}) %all-to-all-start.1) | async-done | bytes 524320 | tf_op jit(solution)/shard_map/all_to_all | solution.py:178
  136.6 0.2 reshape.281
  136.9 0.3 fusion.46
  137.2 0.9 fusion.6
  138.1 0.4 convert_element_type.104
  138.5 1.2 copy.82
  139.7 4.8 %all-to-all-start.2 = ((bf16[4,128,1,2,256]{4,3,1,2,0:T(2,128)(2,1)}), bf16[4,128,1,2,256]{4,3,1,2,0:T(2,128)(2,1)S(1)}, u32[]{:S(2)}, u32[]{:S(2)}) async-start(bf16[4,128,1,2,256]{4,3,1,2,0:T(2,128)(2,1)} %bitcast.80), calls=%async_computation.2 | async-start | bytes 1048576 | tf_op jit(solution)/shard_map/all_to_all | solution.py:35
  144.5 0.1 fusion.45
  144.6 0.2 select_reduce_fusion
  144.8 9.5 %all-to-all-done.2 = bf16[4,128,1,2,256]{4,3,1,2,0:T(2,128)(2,1)S(1)} async-done(((bf16[4,128,1,2,256]{4,3,1,2,0:T(2,128)(2,1)}), bf16[4,128,1,2,256]{4,3,1,2,0:T(2,128)(2,1)S(1)}, u32[]{:S(2)}, u32[]{:S(2)}) %all-to-all-start.2) | async-done | bytes 524320 | tf_op jit(solution)/shard_map/all_to_all | solution.py:35
  154.4 1.3 reduce_sum.121
  155.7 6.8 %all-to-all-start.3 = ((bf16[128,1,2,256]{3,2,1,0:T(2,128)(2,1)}), bf16[128,1,2,256]{3,2,1,0:T(2,128)(2,1)S(1)}, u32[]{:S(2)}, u32[]{:S(2)}) async-start(bf16[128,1,2,256]{3,2,1,0:T(2,128)(2,1)} %bitcast.7), calls=%async_computation.3 | async-start | bytes 262144 | tf_op jit(solution)/shard_map/all_to_all | solution.py:191
  162.5 0.1 copy.69
  162.6 0.1 multiply_reduce_fusion.2
  162.7 0.1 fusion.21
  162.8 2.2 copy.81
  165.0 0.4 reshape_reshape.7
  165.5 13.3 %all-to-all-done.3 = bf16[128,1,2,256]{3,2,1,0:T(2,128)(2,1)S(1)} async-done(((bf16[128,1,2,256]{3,2,1,0:T(2,128)(2,1)}), bf16[128,1,2,256]{3,2,1,0:T(2,128)(2,1)S(1)}, u32[]{:S(2)}, u32[]{:S(2)}) %all-to-all-start.3) | async-done | bytes 131104 | tf_op jit(solution)/shard_map/all_to_all | solution.py:191
  178.8 0.1 fusion.37
  179.0 71.2 %all-gather.5.cloned.1.call-done = bf16[1024,1024]{1,0:T(8,128)(2,1)} async-done(((bf16[8,1024]{1,0:T(8,128)(2,1)}), bf16[1024,1024]{1,0:T(8,128)(2,1)}) %all-gather.5.cloned.1.call-update) | async-done | bytes 2097168 | tf_op jit(solution)/shard_map/all_gather | solution.py:206
  250.1 2.4 fusion.47
  252.6 0.7 fusion.8
  253.2 0.9 copy.71
  254.1 12.4 %all-to-all-start.4 = ((bf16[128,8,22]{2,1,0:T(8,128)(2,1)}), bf16[128,8,22]{2,1,0:T(8,128)(2,1)S(1)}, u32[]{:S(2)}, u32[]{:S(2)}) async-start(bf16[128,8,22]{2,1,0:T(8,128)(2,1)} %bitcast.9), calls=%async_computation.4 | async-start | bytes 524288 | tf_op jit(solution)/shard_map/all_to_all | solution.py:210
  266.5 0.1 convolution_add_fusion
  266.6 21.5 %all-to-all-done.4 = bf16[128,8,22]{2,1,0:T(8,128)(2,1)S(1)} async-done(((bf16[128,8,22]{2,1,0:T(8,128)(2,1)}), bf16[128,8,22]{2,1,0:T(8,128)(2,1)S(1)}, u32[]{:S(2)}, u32[]{:S(2)}) %all-to-all-start.4) | async-done | bytes 45088 | tf_op jit(solution)/shard_map/all_to_all | solution.py:210
  288.2 0.3 all_to_all.37
  288.5 0.4 fusion.44
  289.0 0.1 pad_maximum_fusion.1
  289.1 0.6 broadcast_in_dim.60
  289.6 4.3 %all-to-all-start.5 = ((f32[4,1,16]{2,1,0:T(1,128)}), f32[4,1,16]{2,1,0:T(1,128)S(1)}, u32[]{:S(2)}, u32[]{:S(2)}) async-start(f32[4,1,16]{2,1,0:T(1,128)} %broadcast_in_dim.60), calls=%async_computation.5 | async-start | bytes 4096 | tf_op jit(solution)/shard_map/all_to_all | solution.py:19
  293.9 0.7 pad_maximum_fusion
  294.6 4.6 %all-to-all-done.5 = f32[4,1,16]{2,1,0:T(1,128)S(1)} async-done(((f32[4,1,16]{2,1,0:T(1,128)}), f32[4,1,16]{2,1,0:T(1,128)S(1)}, u32[]{:S(2)}, u32[]{:S(2)}) %all-to-all-start.5) | async-done | bytes 288 | tf_op jit(solution)/shard_map/all_to_all | solution.py:19
  299.1 0.1 slice_multiply_fusion
  299.2 0.7 multiply_convert_fusion.1
  (67 shorter events, 0.9 us)
Async XLA Ops:
  7.2 26.3 %copy-start = (bf16[128,1024]{1,0:T(8,128)(2,1)S(1)}, bf16[128,1024]{1,0:T(8,128)(2,1)}, u32[]{:S(2)}) copy-start(bf16[128,1024]{1,0:T(8,128)(2,1)} %param.28) | copy-start | bytes 786436
  7.2 25.0 %copy-start.16 = (bf16[8,1,1024,128]{3,2,1,0:T(8,128)(2,1)S(1)}, bf16[8,1,1024,128]{3,2,1,0:T(8,128)(2,1)}, u32[]{:S(2)}) copy-start(bf16[8,1,1024,128]{3,2,1,0:T(8,128)(2,1)} %param.21) | copy-start | bytes 6291460
  32.0 1.6 copy-start.15
  32.2 6.6 %copy-start.10 = (bf16[22,256]{1,0:T(8,128)(2,1)S(1)}, bf16[22,256]{1,0:T(8,128)(2,1)}, u32[]{:S(2)}) copy-start(bf16[22,256]{1,0:T(8,128)(2,1)} %param.37) | copy-start | bytes 33796
  33.3 56.1 %copy-start.12 = (s32[8,2]{0,1:T(2,128)S(1)}, s32[8,2]{0,1:T(2,128)}, u32[]{:S(2)}) copy-start(s32[8,2]{0,1:T(2,128)} %param.31) | copy-start | bytes 196
  33.3 56.6 %copy-start.2 = (bf16[8,1024]{1,0:T(8,128)(2,1)S(1)}, bf16[8,1024]{1,0:T(8,128)(2,1)}, u32[]{:S(2)}) copy-start(bf16[8,1024]{1,0:T(8,128)(2,1)} %param.20) | copy-start | bytes 49156
  33.3 57.0 %copy-start.11 = (f32[1024]{0:T(1024)S(1)}, f32[1024]{0:T(1024)}, u32[]{:S(2)}) copy-start(f32[1024]{0:T(1024)} %param.29) | copy-start | bytes 12292
  34.3 55.6 %all-to-all-start = ((bf16[4,8,1024]{2,1,0:T(8,128)(2,1)}), bf16[4,8,1024]{2,1,0:T(8,128)(2,1)S(1)}, u32[]{:S(2)}, u32[]{:S(2)}) async-start(bf16[4,8,1024]{2,1,0:T(8,128)(2,1)} %broadcast_in_dim.35), calls=%async_computation | async-start | bytes 131072 | tf_op jit(solution)/shard_map/all_to_all | solution.py:19
  38.8 124.0 %all-gather.7.cloned.1.call-start = ((), (), s32[]{:S(2)}) async-start(), calls=%async_computation.7 | async-start | bytes 2162688 | tf_op jit(solution)/shard_map/all_gather | solution.py:48
  75.2 28.8 %copy-start.5 = (bf16[1024,64]{0,1:T(8,128)(2,1)S(1)}, bf16[1024,64]{0,1:T(8,128)(2,1)}, u32[]{:S(2)}) copy-start(bf16[1024,64]{0,1:T(8,128)(2,1)} %param.24) | copy-start | bytes 393220
  75.3 29.0 %copy-start.6 = (bf16[1024,64]{0,1:T(8,128)(2,1)S(1)}, bf16[1024,64]{0,1:T(8,128)(2,1)}, u32[]{:S(2)}) copy-start(bf16[1024,64]{0,1:T(8,128)(2,1)} %param.25) | copy-start | bytes 393220
  89.3 47.5 %copy-start.4 = (bf16[1024,112]{0,1:T(8,128)(2,1)S(1)}, bf16[1024,112]{0,1:T(8,128)(2,1)}, u32[]{:S(2)}) copy-start(bf16[1024,112]{0,1:T(8,128)(2,1)} %param.32) | copy-start | bytes 688132
  89.4 160.8 %all-gather.5.cloned.1.call-start = ((), (), s32[]{:S(2)}) async-start(), calls=%async_computation.6 | async-start | bytes 2113536 | tf_op jit(solution)/shard_map/all_gather | solution.py:206
  91.3 45.9 %copy-start.17 = (bf16[112,1024]{1,0:T(8,128)(2,1)S(1)}, bf16[112,1024]{1,0:T(8,128)(2,1)}, u32[]{:S(2)}) copy-start(bf16[112,1024]{1,0:T(8,128)(2,1)} %param.34) | copy-start | bytes 688132
  91.3 45.9 %copy-start.18 = (bf16[1024,112]{0,1:T(8,128)(2,1)S(1)}, bf16[1024,112]{0,1:T(8,128)(2,1)}, u32[]{:S(2)}) copy-start(bf16[1024,112]{0,1:T(8,128)(2,1)} %param.33) | copy-start | bytes 688132
  93.4 43.2 %all-to-all-start.1 = ((bf16[128,1,2,1024]{3,2,1,0:T(2,128)(2,1)}), bf16[128,1,2,1024]{3,2,1,0:T(2,128)(2,1)S(1)}, u32[]{:S(2)}, u32[]{:S(2)}) async-start(bf16[128,1,2,1024]{3,2,1,0:T(2,128)(2,1)} %bitcast.5), calls=%async_computation.1 | async-start | bytes 1048576 | tf_op jit(solution)/shard_map/all_to_all | solution.py:178
  137.2 7.3 %copy-start.13 = (bf16[1024]{0:T(1024)(128)(2,1)S(1)}, bf16[1024]{0:T(1024)(128)(2,1)}, u32[]{:S(2)}) copy-start(bf16[1024]{0:T(1024)(128)(2,1)} %param.38) | copy-start | bytes 6148
  137.2 7.3 %copy-start.3 = (bf16[8,1024]{1,0:T(8,128)(2,1)S(1)}, bf16[8,1024]{1,0:T(8,128)(2,1)}, u32[]{:S(2)}) copy-start(bf16[8,1024]{1,0:T(8,128)(2,1)} %multiply_convert_fusion) | copy-start | bytes 49156
  137.2 7.3 %copy-start.9 = (bf16[1024,16]{0,1:T(8,128)(2,1)S(1)}, bf16[1024,16]{0,1:T(8,128)(2,1)}, u32[]{:S(2)}) copy-start(bf16[1024,16]{0,1:T(8,128)(2,1)} %param.30) | copy-start | bytes 98308
  139.7 14.7 %all-to-all-start.2 = ((bf16[4,128,1,2,256]{4,3,1,2,0:T(2,128)(2,1)}), bf16[4,128,1,2,256]{4,3,1,2,0:T(2,128)(2,1)S(1)}, u32[]{:S(2)}, u32[]{:S(2)}) async-start(bf16[4,128,1,2,256]{4,3,1,2,0:T(2,128)(2,1)} %bitcast.80), calls=%async_computation.2 | async-start | bytes 1048576 | tf_op jit(solution)/shard_map/all_to_all | solution.py:35
  155.7 23.1 %all-to-all-start.3 = ((bf16[128,1,2,256]{3,2,1,0:T(2,128)(2,1)}), bf16[128,1,2,256]{3,2,1,0:T(2,128)(2,1)S(1)}, u32[]{:S(2)}, u32[]{:S(2)}) async-start(bf16[128,1,2,256]{3,2,1,0:T(2,128)(2,1)} %bitcast.7), calls=%async_computation.3 | async-start | bytes 262144 | tf_op jit(solution)/shard_map/all_to_all | solution.py:191
  165.0 85.2 %copy-start.7 = (bf16[1024,22]{0,1:T(8,128)(2,1)S(1)}, bf16[1024,22]{0,1:T(8,128)(2,1)}, u32[]{:S(2)}) copy-start(bf16[1024,22]{0,1:T(8,128)(2,1)} %param.35) | copy-start | bytes 135172
  165.4 87.1 %copy-start.8 = (bf16[1024,22]{0,1:T(8,128)(2,1)S(1)}, bf16[1024,22]{0,1:T(8,128)(2,1)}, u32[]{:S(2)}) copy-start(bf16[1024,22]{0,1:T(8,128)(2,1)} %param.36) | copy-start | bytes 135172
  250.1 2.4 copy-start.1
  253.2 46.0 %copy-start.14 = (f32[256]{0:T(256)S(1)}, f32[256]{0:T(256)}, u32[]{:S(2)}) copy-start(f32[256]{0:T(256)} %param.39) | copy-start | bytes 3076
  254.1 34.1 %all-to-all-start.4 = ((bf16[128,8,22]{2,1,0:T(8,128)(2,1)}), bf16[128,8,22]{2,1,0:T(8,128)(2,1)S(1)}, u32[]{:S(2)}, u32[]{:S(2)}) async-start(bf16[128,8,22]{2,1,0:T(8,128)(2,1)} %bitcast.9), calls=%async_computation.4 | async-start | bytes 524288 | tf_op jit(solution)/shard_map/all_to_all | solution.py:210
  289.6 9.5 %all-to-all-start.5 = ((f32[4,1,16]{2,1,0:T(1,128)}), f32[4,1,16]{2,1,0:T(1,128)S(1)}, u32[]{:S(2)}, u32[]{:S(2)}) async-start(f32[4,1,16]{2,1,0:T(1,128)} %broadcast_in_dim.60), calls=%async_computation.5 | async-start | bytes 4096 | tf_op jit(solution)/shard_map/all_to_all | solution.py:19
Sparse Core Ops, SparseCore 0:
  89.5 16.0 all-gather.6
  108.7 141.3 all-gather.4
where the time goes:
time: 308 us; the launch traced here: 307 us
  waiting for transfers between devices  152 us (49%)
  blocking collectives  50.5 us (16%)
  starting transfers between devices  43.4 us (14%)
  other arithmetic  25.7 us (8%)
  between operations  14.5 us (5%)
  matrix products  11.1 us (4%)
  local copies, waits for them, and re-layouts  9.17 us (3%)
    all_gather x1, waiting for transfers between devices, body(): shard_rows = lax.all_gather(settled, EP, axis=0, tiled=True)  71.2 us
    all_gather x2, blocking collectives, stacked_from(): tiles = lax.all_gather(tiles, axes[k], axis=0, tiled=True)  50.5 us
    all_to_all x1, waiting for transfers between devices, body(): lax.all_to_all(outgoing, EP, split_axis=0, concat_axis=0, tiled=True)  32.3 us
    all_to_all x1, waiting for transfers between devices, body(): lax.all_to_all(dense_hidden, EP, split_axis=0, concat_axis=1, tiled=True)  21.5 us
    another operation x2, other arithmetic  20.1 us
    all_to_all x1, waiting for transfers between devices, body(): lax.all_to_all(summed.astype(jnp.bfloat16), EP, split_axis=0, concat_axis...  13.3 us
    all_to_all x1, starting transfers between devices, body(): lax.all_to_all(dense_hidden, EP, split_axis=0, concat_axis=1, tiled=True)  12.4 us
    all_to_all x1, starting transfers between devices, body(): lax.all_to_all(outgoing, EP, split_axis=0, concat_axis=0, tiled=True)  10.6 us
  transfers between devices with their start and end apart: 8, of which 6 were waited for; matrix products, arithmetic and copies ran while one was open for 4% of the time, Pallas kernels for 0%

commit v1 on v0

v1 whole, which is shorter than its diff:
```python
import functools

import jax
import jax.numpy as jnp
from jax import lax
from jax.experimental import pallas as pl
from jax.experimental.pallas import tpu as pltpu
from jax.sharding import Mesh
from jax.sharding import PartitionSpec as P

CAP = 2
EP = ("ep_0", "ep_1", "ep_2")
EP_TP = ("ep_0", "ep_1", "ep_2", "tp")
RESIDUAL_SCALE = 8.0**0.25
MESH = pl.DeviceIdType.MESH
F32 = jnp.float32
BF16 = jnp.bfloat16


def nt(a, b):
    return lax.dot_general(a, b, (((1,), (1,)), ((), ())), preferred_element_type=F32)


def nn(a, b):
    return jnp.dot(a, b, preferred_element_type=F32)


def iota(shape, dim):
    return lax.broadcasted_iota(jnp.int32, shape, dim)


def layer_kernel(
    dims,
    tokens_hbm,
    kv_hbm,
    lengths_ref,
    wq_hbm,
    wk_hbm,
    wv_hbm,
    bias_ref,
    head_gain_ref,
    wo_hbm,
    attn_gain_ref,
    router_hbm,
    routes_ref,
    eg_hbm,
    eu_hbm,
    ed_hbm,
    dg_hbm,
    du_hbm,
    dd_hbm,
    mix_ref,
    ffn_gain_ref,
    out_ref,
    new_kv_ref,
    tok,
    kv,
    wq,
    wkv,
    wo,
    router,
    wg,
    wu,
    wd,
    dg_in,
    du_in,
    dd_in,
    dw,
    att,
    settled_cols,
    rows,
    info,
    xe,
    pb,
    pr,
    fb,
    fr,
    stats,
    load_sem,
    kv_sem,
    weight_sem,
    send_sem,
    recv_sem,
):
    Z, X, C, Y = dims
    z, x, c, y = (lax.axis_index(a) for a in EP_TP)
    T, D = tok.shape
    DY = D // Y
    L = kv.shape[1]
    HD = kv.shape[2] // 2
    XC = X * C
    xc = x * C + c
    other = 1 - c
    sib = (z, x, other, y)

    loads = {}

    def load(name, k, src, dst):
        loads[name] = pltpu.make_async_copy(src, dst, load_sem.at[k])
        loads[name].start()

    load("tok", 0, tokens_hbm, tok)
    load("wq", 1, wq_hbm, wq)
    load("wk", 2, wk_hbm, wkv.at[0])
    load("wv", 3, wv_hbm, wkv.at[1])
    kv_copies = [pltpu.make_async_copy(kv_hbm.at[b], kv.at[b], kv_sem.at[b]) for b in range(T)]
    for copy in kv_copies:
        copy.start()
    load("dg", 4, dg_hbm, dg_in)
    load("du", 5, du_hbm, du_in)
    load("dd", 6, dd_hbm, dd_in)
    load("wo", 7, wo_hbm, wo)
    load("router", 8, router_hbm, router)
    load("eg", 9, eg_hbm, wg.at[c])
    load("eu", 10, eu_hbm, wu.at[c])
    load("ed", 11, ed_hbm, wd.at[c])

    barrier = pltpu.get_barrier_semaphore()

    def tell(device):
        pl.semaphore_signal(barrier, inc=1, device_id=device, device_id_type=MESH)

    def far_first(i):
        half = Z // 2
        step = (i + 1) // 2
        return lax.rem(z + half + step * (1 - 2 * lax.rem(i, 2)) + Z, Z)

    def tell_line(i, _):
        tell((far_first(i), x, c, y))
        return 0

    lax.fori_loop(0, Z - 1, tell_line, 0)
    plane = [(i, j) for i in range(X) for j in range(Y) if (i, j) != (0, 0)]

    def plane_peer(i, j):
        return lax.rem(x + i, X), lax.rem(y + j, Y)

    for i, j in plane:
        px, py = plane_peer(i, j)
        tell((z, px, c, py))
    for i in range(X):
        tell((z, lax.rem(x + i, X), other, y))
    partners = Z - 1 + X * Y - 1 + X

    loads["tok"].wait()
    loads["wq"].wait()
    tokens = tok[...]
    queries = nn(tokens, wq[...]).astype(BF16).astype(F32)
    lane = iota((T, 2 * HD), 1)
    turned = pltpu.roll(queries, HD, 1)
    both = jnp.concatenate(
        [jnp.where(lane < HD, queries, 0.0), jnp.where(lane < HD, turned, 0.0)], axis=0
    ).astype(BF16)
    loads["wk"].wait()
    loads["wv"].wait()
    new_kv_ref[...] = nt(tokens, wkv[...].reshape(2 * HD, D)).astype(BF16)

    R = 2 * T
    row_seq = lax.rem(iota((R, 1), 0), T)
    scores = jnp.zeros((R, L), F32)
    limit = jnp.zeros((R, 1), jnp.int32)
    for b in range(T):
        kv_copies[b].wait()
        scores = jnp.where(row_seq == b, nt(both, kv[b]), scores)
        limit = jnp.where(row_seq == b, lengths_ref[b], limit)
    bias = jnp.where(iota((R, 1), 0) < T, bias_ref[0], bias_ref[1])
    scores = scores * HD ** (-0.5) + bias
    tail = jnp.log1p(jnp.exp(-jnp.abs(scores)))
    visible = iota((R, L), 1) < limit
    survive = jnp.where(visible, jnp.minimum(-scores, 0.0) - tail, 0.0)
    taken = jnp.minimum(scores, 0.0) - tail
    blocks = L // 128
    left = jnp.concatenate([survive[:, k * 128 : (k + 1) * 128] for k in range(blocks)], axis=0)
    later = jnp.where(
        (iota((128, 256), 1) >= 128) | (iota((128, 256), 0) > iota((128, 256), 1)), 1.0, 0.0
    ).astype(BF16)
    sums = jnp.zeros((blocks * R, 256), F32)
    for _ in range(3):
        piece = left.astype(BF16)
        sums = sums + nn(piece, later)
        left = left - piece.astype(F32)
    beyond = jnp.zeros((R, 128), F32)
    parts = []
    for k in reversed(range(blocks)):
        here = slice(k * R, (k + 1) * R)
        span = slice(k * 128, (k + 1) * 128)
        parts.append(
            jnp.where(
                visible[:, span], jnp.exp(taken[:, span] + (sums[here, :128] + beyond)), 0.0
            )
        )
        beyond = beyond + sums[here, 128:]
    weights = jnp.concatenate(parts[::-1], axis=1).astype(BF16)
    blended = jnp.zeros((R, 2 * HD), F32)
    for b in range(T):
        blended = jnp.where(row_seq == b, nn(weights, kv[b]), blended)
    wide = iota((R, 2 * HD), 1)
    square = jnp.sum(jnp.where(wide >= HD, blended * blended, 0.0), axis=1, keepdims=True)
    blended = blended * lax.rsqrt(square / HD + 1e-06)
    heads = jnp.where(lane < HD, pltpu.roll(blended[:T], HD, 1), blended[T:])
    normed = (heads * head_gain_ref[...]).astype(BF16)
    loads["wo"].wait()
    att[y] = nn(normed, wo[...]).astype(BF16)

    pl.semaphore_wait(barrier, partners)

    def send(src, dst, k, device):
        pltpu.make_async_remote_copy(
            src_ref=src,
            dst_ref=dst,
            send_sem=send_sem.at[k],
            recv_sem=recv_sem.at[k],
            device_id=device,
            device_id_type=MESH,
        ).start()

    def arrived(ref, k):
        pltpu.make_async_copy(ref, ref, recv_sem.at[k]).wait()

    def left_here(ref, k):
        pltpu.make_async_copy(ref, ref, send_sem.at[k]).wait()

    for j in range(1, Y):
        send(att.at[y], att.at[y], 0, (z, x, c, lax.rem(y + j, Y)))
    for name in ("eg", "eu", "ed"):
        loads[name].wait()
    send(wg.at[c], wg.at[c], 1, sib)
    send(wu.at[c], wu.at[c], 2, sib)
    send(wd.at[c], wd.at[c], 3, sib)
    for name in ("dg", "du", "dd"):
        loads[name].wait()
    FD = dg_in.shape[0]
    FDP = dw.shape[1]

    def padded(values):
        spare = jnp.zeros((FDP - FD, values.shape[1]), F32)
        return jnp.concatenate([values.astype(F32), spare], axis=0).astype(BF16)

    dw[xc, :, :D] = padded(dg_in[...])
    dw[xc, :, D : 2 * D] = padded(du_in[...])
    dw[xc, :, 2 * D :] = padded(dd_in[...])
    for i in range(X):
        for j in range(C):
            if (i, j) != (0, 0):
                send(dw.at[xc], dw.at[xc], 4, (z, lax.rem(x + i, X), lax.rem(c + j, C), y))

    arrived(att.at[pl.ds(0, Y - 1)], 0)
    attended = att[0].astype(F32)
    for j in range(1, Y):
        attended = attended + att[j].astype(F32)
    gain = jnp.concatenate([attn_gain_ref[k : k + 1, :] for k in range(D // 128)], axis=1)
    values = RESIDUAL_SCALE * tokens.astype(F32) + attended
    centred = values - jnp.mean(values, axis=1, keepdims=True)
    spread = jnp.mean(centred * centred, axis=1, keepdims=True)
    settled = (centred * lax.rsqrt(spread + 1e-05) * gain).astype(BF16)
    for j in range(Y):
        settled_cols[j] = settled[:, j * DY : (j + 1) * DY]
    rows[y, z] = settled_cols[y]

    def send_rows(i, _):
        send(rows.at[y, z], rows.at[y, z], 5, (far_first(i), x, c, y))
        return 0

    lax.fori_loop(0, Z - 1, send_rows, 0)

    loads["router"].wait()
    logits = nt(settled, router[...])
    experts = logits.shape[1]
    mix_row = jnp.concatenate(
        [mix_ref[k : k + 1, :].astype(F32) for k in range(D // 128)], axis=1
    )
    mix = 1.0 / (
        1.0 + jnp.exp(-jnp.sum(settled.astype(F32) * mix_row, axis=1, keepdims=True))
    )
    token_row = iota((T, 1), 0)
    routes = []
    for j in range(2):
        column = jnp.zeros((T, 1), jnp.int32)
        for t in range(T):
            column = jnp.where(token_row == t, routes_ref[j, t], column)
        routes.append(column)
    small = iota((T, experts), 1)
    picked = [
        jnp.sum(jnp.where(small == r, logits, 0.0), axis=1, keepdims=True) for r in routes
    ]
    share = [1.0 / (1.0 + jnp.exp(picked[1 - j] - picked[j])) for j in range(2)]
    lanes = iota((T, 128), 1)
    lane_expert = lax.rem(lanes, experts)
    lane_group = lanes // experts
    hits = [lane_expert == r for r in routes]
    named = jnp.where(hits[0] | hits[1], 1.0, 0.0)
    before = jnp.zeros((T, 128), F32)
    for t in range(T - 1):
        before = before + jnp.where(token_row > t, named[t : t + 1, :], 0.0)
    lane_slot = lax.rem(lane_group, 2).astype(F32)
    placed = jnp.where(before == lane_slot, named, 0.0)
    placed_share = placed * jnp.where(hits[0], share[0], share[1])

    def high(v):
        return v.astype(BF16).astype(F32)

    share_high = high(placed_share)
    mix_high = high(mix)
    table = jnp.where(
        lane_group < 2, placed, jnp.where(lane_group < 4, share_high, placed_share - share_high)
    )
    table = jnp.where(
        lanes < 6 * experts,
        table,
        jnp.where(
            lanes == 6 * experts,
            mix_high,
            jnp.where(lanes == 6 * experts + 1, mix - mix_high, 0.0),
        ),
    )
    info[z] = table.astype(BF16)

    def send_info(i, _):
        send(info.at[z], info.at[z], 6, (far_first(i), x, c, y))
        return 0

    lax.fori_loop(0, Z - 1, send_info, 0)

    ZT = Z * T
    ZS = Z * CAP
    arrived(info.at[pl.ds(0, Z - 1)], 6)
    facts = info[...].astype(F32).reshape(ZT, 128).astype(BF16)
    sel_row = iota((ZS, 128), 0)
    sel_pick = jnp.where(iota((ZS, 128), 1) == lax.rem(sel_row, CAP) * experts + z, 1.0, 0.0)
    select = nt(sel_pick.astype(BF16), facts)
    select = jnp.where(
        iota((ZS, ZT), 0) // CAP == iota((ZS, ZT), 1) // T, select, 0.0
    ).astype(BF16)
    share_row = iota((3 * ZS, 128), 0)
    share_group = jnp.where(share_row < 2 * ZS, 2, 4) + lax.rem(share_row, CAP)
    share_pick = jnp.where(iota((3 * ZS, 128), 1) == share_group * experts + z, 1.0, 0.0)
    shares = nt(facts, share_pick.astype(BF16))
    shares = jnp.where(
        iota((ZT, 3 * ZS), 0) // T == lax.rem(iota((ZT, 3 * ZS), 1), ZS) // CAP, shares, 0.0
    ).astype(BF16)
    fact_lane = iota((ZT, 128), 1)
    mixes = jnp.sum(
        jnp.where(
            (fact_lane == 6 * experts) | (fact_lane == 6 * experts + 1), facts.astype(F32), 0.0
        ),
        axis=1,
        keepdims=True,
    )
    arrived(rows.at[y, pl.ds(0, Z - 1)], 5)
    own_rows = rows[y].astype(F32).reshape(ZT, DY).astype(BF16)
    seat = y * X + x
    xe[seat] = nn(select, own_rows).astype(BF16)
    for i, j in plane:
        px, py = plane_peer(i, j)
        send(xe.at[seat], xe.at[seat], 7, (z, px, c, py))
    for j in range(1, Y):
        send(rows.at[y], rows.at[y], 8, (z, x, c, lax.rem(y + j, Y)))

    arrived(wg.at[0], 1)
    arrived(wu.at[0], 2)
    arrived(wd.at[0], 3)
    F = 2 * wg.shape[1]
    gate_t = wg[...].reshape(F, D)
    up_t = wu[...].reshape(F, D)
    down = wd[...].reshape(F, D)
    arrived(xe.at[pl.ds(0, X * Y - 1)], 7)
    received = jnp.concatenate(
        [xe[j * X : (j + 1) * X].reshape(X * ZS, DY) for j in range(Y)], axis=1
    )
    gate_pre = nt(received, gate_t)
    up_pre = nt(received, up_t)
    hidden = (gate_pre / (1.0 + jnp.exp(-gate_pre)) * up_pre).astype(BF16)
    partial = nn(hidden, down).astype(BF16)
    for i in range(X):
        for j in range(Y):
            pb[j * X + i] = partial[i * ZS : (i + 1) * ZS, j * DY : (j + 1) * DY]
    for i, j in plane:
        px, py = plane_peer(i, j)
        send(pb.at[py * X + px], pr.at[seat], 9, (z, px, c, py))
    pr[seat] = pb[seat]

    arrived(dw.at[pl.ds(0, XC - 1)], 4)
    arrived(rows.at[pl.ds(0, Y - 1)], 8)
    FP = XC * FDP
    line = jnp.concatenate(
        [rows[j].astype(F32).reshape(ZT, DY).astype(BF16) for j in range(Y)], axis=1
    )

    def stacked(a, b):
        return jnp.concatenate([dw[k, :, a:b] for k in range(XC)], axis=0)

    dense_gate = nt(line, stacked(0, D))
    dense_up = nt(line, stacked(D, 2 * D))
    dense_hidden = (dense_gate / (1.0 + jnp.exp(-dense_gate)) * dense_up).astype(BF16)
    dense = nn(dense_hidden, stacked(2 * D, 2 * D + DY)) * mixes

    arrived(pr.at[pl.ds(0, X * Y - 1)], 9)
    served = jnp.zeros((ZS, DY), F32)
    for k in range(X * Y):
        served = served + pr[k].astype(F32)
    served_high = served.astype(BF16)
    served_low = (served - served_high.astype(F32)).astype(BF16)
    stack = jnp.concatenate([served_high, served_low, served_high], axis=0)
    mixed = dense + nn(shares, stack)
    fb[...] = mixed.reshape(Z, T, DY).astype(BF16)
    fr[z] = fb[z]

    def send_back(i, _):
        to = far_first(i)
        send(fb.at[to], fr.at[z], 10, (to, x, c, y))
        return 0

    lax.fori_loop(0, Z - 1, send_back, 0)

    arrived(fr.at[pl.ds(0, Z - 1)], 10)
    combined = RESIDUAL_SCALE * settled_cols[y].astype(F32)
    combined = combined + jnp.sum(fr[...].astype(F32), axis=0)
    centre = jnp.sum(combined, axis=1, keepdims=True) / DY
    centred = combined - centre
    scatter = jnp.sum(centred * centred, axis=1, keepdims=True)
    stats[y] = jnp.where(lanes == 0, centre, jnp.where(lanes == 1, scatter, 0.0))
    for j in range(1, Y):
        send(stats.at[y], stats.at[y], 11, (z, x, c, lax.rem(y + j, Y)))
    ffn_gain = jnp.concatenate(
        [ffn_gain_ref[k : k + 1, :] for k in range(DY // 128)], axis=1
    )
    arrived(stats.at[pl.ds(0, Y - 1)], 11)
    every = [stats[j] for j in range(Y)]
    mean = sum(e[:, 0:1] for e in every) / Y
    var = sum(e[:, 1:2] + DY * (e[:, 0:1] - mean) * (e[:, 0:1] - mean) for e in every) / D
    out_ref[...] = ((combined - mean) * lax.rsqrt(var + 1e-05) * ffn_gain).astype(BF16)

    left_here(att.at[pl.ds(0, Y - 1)], 0)
    left_here(wg.at[0], 1)
    left_here(wu.at[0], 2)
    left_here(wd.at[0], 3)
    left_here(dw.at[pl.ds(0, XC - 1)], 4)
    left_here(rows.at[y, pl.ds(0, Z - 1)], 5)
    left_here(info.at[pl.ds(0, Z - 1)], 6)
    left_here(xe.at[pl.ds(0, X * Y - 1)], 7)
    left_here(rows.at[pl.ds(0, Y - 1)], 8)
    left_here(pb.at[pl.ds(0, X * Y - 1)], 9)
    left_here(fb.at[pl.ds(0, Z - 1)], 10)
    left_here(stats.at[pl.ds(0, Y - 1)], 11)


def body(
    dims,
    tokens,
    kv_cache,
    lengths,
    w_query,
    w_key,
    w_value,
    break_bias,
    head_gain,
    w_output,
    attn_norm_gain,
    w_router,
    routes,
    expert_gate,
    expert_up,
    expert_down,
    dense_gate,
    dense_up,
    dense_down,
    mix_gate,
    ffn_norm_gain,
):
    Z, X, C, Y = dims
    T, D = tokens.shape
    DY = D // Y
    L, HD2 = kv_cache.shape[2:]
    F = expert_gate.shape[1]
    FD = dense_gate.shape[1]
    FDP = -(-FD // 8) * 8
    ZS = Z * CAP
    experts = w_router.shape[1]
    anywhere = pl.BlockSpec(memory_space=pl.ANY)
    vmem = pl.BlockSpec(memory_space=pltpu.VMEM)
    smem = pl.BlockSpec(memory_space=pltpu.SMEM)
    V = pltpu.VMEM
    result, new_kv = pl.pallas_call(
        functools.partial(layer_kernel, dims),
        out_shape=(
            jax.ShapeDtypeStruct((T, DY), BF16),
            jax.ShapeDtypeStruct((T, HD2), BF16),
        ),
        in_specs=[
            anywhere,
            anywhere,
            smem,
            anywhere,
            anywhere,
            anywhere,
            smem,
            vmem,
            anywhere,
            vmem,
            anywhere,
            smem,
            anywhere,
            anywhere,
            anywhere,
            anywhere,
            anywhere,
            anywhere,
            vmem,
            vmem,
        ],
        out_specs=(vmem, vmem),
        scratch_shapes=[
            V((T, D), BF16),
            V((T, L, HD2), BF16),
            V((D, HD2), BF16),
            V((2, HD2 // 2, D), BF16),
            V((HD2, D), BF16),
            V((experts, D), BF16),
            V((C, F, D), BF16),
            V((C, F, D), BF16),
            V((C, F, D), BF16),
            V((FD, D), BF16),
            V((FD, D), BF16),
            V((FD, DY), BF16),
            V((X * C, FDP, 2 * D + DY), BF16),
            V((Y, T, D), BF16),
            V((Y, T, DY), BF16),
            V((Y, Z, T, DY), BF16),
            V((Z, T, 128), BF16),
            V((X * Y, ZS, DY), BF16),
            V((X * Y, ZS, DY), BF16),
            V((X * Y, ZS, DY), BF16),
            V((Z, T, DY), BF16),
            V((Z, T, DY), BF16),
            V((Y, T, 128), F32),
            pltpu.SemaphoreType.DMA((12,)),
            pltpu.SemaphoreType.DMA((T,)),
            pltpu.SemaphoreType.DMA((2,)),
            pltpu.SemaphoreType.DMA((12,)),
            pltpu.SemaphoreType.DMA((12,)),
        ],
        compiler_params=pltpu.CompilerParams(
            collective_id=0, has_side_effects=True, vmem_limit_bytes=67043328
        ),
        name="layer",
    )(
        tokens,
        kv_cache.reshape(T, L, HD2),
        lengths,
        w_query,
        w_key.T,
        w_value.T,
        break_bias,
        head_gain.reshape(1, HD2),
        w_output,
        attn_norm_gain.reshape(D // 128, 128),
        w_router.T,
        routes.T,
        expert_gate.T,
        expert_up.T,
        expert_down,
        dense_gate.T,
        dense_up.T,
        dense_down,
        mix_gate.reshape(D // 128, 128),
        ffn_norm_gain.reshape(DY // 128, 128),
    )
    return result, new_kv.reshape(T, 1, HD2)


def solution(mesh):
    cores = 2
    ep, tp = mesh.shape["ep"], mesh.shape["tp"]
    dims = (ep // (4 * cores), 4, cores, tp)
    split = Mesh(mesh.devices.reshape(dims), EP_TP)
    return jax.shard_map(
        functools.partial(body, dims),
        mesh=split,
        in_specs=(
            P(EP, None),
            P(EP, "tp", None, None),
            P(EP),
            P(None, "tp"),
            P(None, "tp"),
            P(None, "tp"),
            P("tp"),
            P("tp"),
            P("tp", None),
            P(),
            P(),
            P(EP, None),
            P(None, EP_TP),
            P(None, EP_TP),
            P(EP_TP, None),
            P(None, EP),
            P(None, EP),
            P(EP, "tp"),
            P(),
            P("tp"),
        ),
        out_specs=(P(EP, "tp"), P(EP, "tp", None)),
        check_vma=False,
    )
```

time: 308 us -> 57.9 us (0.19)
  the two profiles are of different devices: /device:TPU:6 before, /device:TPU:32 now
where the time goes in v1:
time: 57.9 us; the launch traced here: 57.6 us
  Pallas kernels  54.4 us (94%)
  local copies, waits for them, and re-layouts  2.5 us (4%)
  between operations  0.65 us (1%)
    pallas_call x1, Pallas kernels, body(): pl.pallas_call(functools.partial(layer_kernel, dims), out_shape=(jax.Shap...  54.4 us
    unnamed x2, local copies, waits for them, and re-layouts  2.5 us

profile of v1, /device:TPU:32, one launch (start us, length us, event | category | flops | bytes accessed | tf_op | source)
XLA Modules:
  0.0 57.6 jit_solution(10554878262888622946)
XLA Ops:
  0.6 54.4 %layer.1 = (bf16[8,256]{1,0:T(8,128)(2,1)}, bf16[8,128]{1,0:T(8,128)(2,1)}) custom-call(bf16[8,1024]{1,0:T(8,128)(2,1)} %tokens_hbm.1, bf16[8,1024,128]{2,1,0:T(8,128)(2,1)} %bitcast.14, s32[8]{0:T(128)} %lengths_ref.1, bf16[1024,128]{1,0:T(8,128)(2,1)} %wq_hbm.1, bf16[64,1024]{1,0:T(8,128)(2,1)} %bitcast.17, bf16[64,1024]{1,0:T(8,128)(2,1)} %bitcast.18, ...), custom_call_target="tpu_custom_call" | custom-call | tf_op jit(solution)/shard_map/layer/pallas_call | solution.py:483
  55.1 1.3 %copy.24 = bf16[8,256]{1,0:T(8,128)(2,1)} copy(bf16[8,256]{1,0:T(8,128)(2,1)} %get-tuple-element.8) | data formatting | bytes 8192
  56.4 1.2 %copy.25 = bf16[8,1,128]{2,0,1:T(8,128)(2,1)} copy(bf16[8,1,128]{2,0,1:T(8,128)(2,1)} %bitcast.24) | data formatting | bytes 4096

commit v2 on v1

v2 whole, which is shorter than its diff:
```python
import functools

import jax
import jax.numpy as jnp
from jax import lax
from jax.experimental import pallas as pl
from jax.experimental.pallas import tpu as pltpu
from jax.sharding import Mesh
from jax.sharding import PartitionSpec as P

CAP = 2
CHUNKS = 2
EP = ("ep_0", "ep_1", "ep_2")
EP_TP = ("ep_0", "ep_1", "ep_2", "tp")
RESIDUAL_SCALE = 8.0**0.25
MESH = pl.DeviceIdType.MESH
F32 = jnp.float32
BF16 = jnp.bfloat16


def nt(a, b):
    return lax.dot_general(a, b, (((1,), (1,)), ((), ())), preferred_element_type=F32)


def nn(a, b):
    return jnp.dot(a, b, preferred_element_type=F32)


def iota(shape, dim):
    return lax.broadcasted_iota(jnp.int32, shape, dim)


def layer_kernel(
    dims,
    tokens_hbm,
    kv_hbm,
    lengths_hbm,
    wq_hbm,
    wk_hbm,
    wv_hbm,
    bias_hbm,
    head_gain_hbm,
    wo_hbm,
    attn_gain_hbm,
    router_hbm,
    routes_hbm,
    eg_hbm,
    eu_hbm,
    ed_hbm,
    dg_hbm,
    du_hbm,
    dd_hbm,
    mix_hbm,
    ffn_gain_hbm,
    out_hbm,
    new_kv_hbm,
    tok,
    kv,
    wq,
    wkv,
    wo,
    router,
    wg,
    wu,
    wd,
    dg_in,
    du_in,
    dd_in,
    dw,
    att,
    settled_cols,
    rows,
    xe,
    pb,
    pr,
    fb,
    fr,
    stats,
    lengths_ref,
    bias_ref,
    routes_ref,
    head_gain_ref,
    attn_gain_ref,
    mix_ref,
    ffn_gain_ref,
    out_ref,
    new_kv_ref,
    load_sem,
    kv_sem,
    send_sem,
    recv_sem,
    hello_line,
    hello_core,
    hello_column,
):
    Z, X, C, Y = dims
    z, x, c, y = (lax.axis_index(a) for a in EP_TP)
    T, D = tok.shape
    DY = D // Y
    L = kv.shape[1]
    HD = kv.shape[2] // 2
    XC = X * C
    xc = x * C + c
    other = 1 - c
    sib = (z, x, other, y)

    loads = {}

    def load(name, k, src, dst):
        loads[name] = pltpu.make_async_copy(src, dst, load_sem.at[k])
        loads[name].start()

    load("tok", 0, tokens_hbm, tok)
    load("wq", 1, wq_hbm, wq)
    load("lengths", 12, lengths_hbm, lengths_ref)
    load("bias", 13, bias_hbm, bias_ref)
    load("wk", 2, wk_hbm, wkv.at[0])
    load("wv", 3, wv_hbm, wkv.at[1])
    kv_copies = [pltpu.make_async_copy(kv_hbm.at[b], kv.at[b], kv_sem.at[b]) for b in range(T)]
    for copy in kv_copies:
        copy.start()
    load("dg", 4, dg_hbm, dg_in)
    load("du", 5, du_hbm, du_in)
    load("dd", 6, dd_hbm, dd_in)
    load("wo", 7, wo_hbm, wo)
    load("router", 8, router_hbm, router)
    load("head_gain", 14, head_gain_hbm, head_gain_ref)
    load("attn_gain", 15, attn_gain_hbm, attn_gain_ref)
    load("routes", 16, routes_hbm, routes_ref)
    load("mix", 17, mix_hbm, mix_ref)
    load("ffn_gain", 18, ffn_gain_hbm, ffn_gain_ref)
    load("eg", 9, eg_hbm, wg.at[c])
    load("eu", 10, eu_hbm, wu.at[c])
    load("ed", 11, ed_hbm, wd.at[c])

    barrier = pltpu.get_barrier_semaphore()

    def tell(sem, device):
        pl.semaphore_signal(sem, inc=1, device_id=device, device_id_type=MESH)

    for j in range(1, Y):
        tell(barrier, (z, x, c, lax.rem(y + j, Y)))
    for i in range(1, X):
        tell(barrier, (z, lax.rem(x + i, X), c, y))

    def tell_later(k, _):
        tell(barrier, (k, x, c, y))
        return 0

    lax.fori_loop(z + 1, Z, tell_later, 0)

    @pl.when(c == 0)
    def _():
        for i in range(X):
            tell(barrier, (z, lax.rem(x + i, X), other, y))

    plane = [(i, j) for i in range(X) for j in range(Y) if (i, j) != (0, 0)]
    plane.sort(key=lambda p: -(min(p[0], X - p[0]) + min(p[1], Y - p[1])))

    def plane_peer(i, j):
        return lax.rem(x + i, X), lax.rem(y + j, Y)

    loads["tok"].wait()
    loads["wq"].wait()
    tokens = tok[...]
    queries = nn(tokens, wq[...]).astype(BF16).astype(F32)
    lane = iota((T, 2 * HD), 1)
    turned = pltpu.roll(queries, HD, 1)
    both = jnp.concatenate(
        [jnp.where(lane < HD, queries, 0.0), jnp.where(lane < HD, turned, 0.0)], axis=0
    ).astype(BF16)
    loads["wk"].wait()
    loads["wv"].wait()
    new_kv_ref[...] = nt(tokens, wkv[...].reshape(2 * HD, D)).astype(BF16)
    put_kv = pltpu.make_async_copy(new_kv_ref, new_kv_hbm, load_sem.at[19])
    put_kv.start()

    loads["lengths"].wait()
    loads["bias"].wait()
    pl.semaphore_wait(barrier, Y - 1 + X - 1 + z + c * X)

    def answer(k, _):
        tell(hello_line.at[z], (k, x, c, y))
        return 0

    lax.fori_loop(0, z, answer, 0)

    @pl.when(c == 1)
    def _():
        for i in range(X):
            tell(hello_core, (z, lax.rem(x + i, X), other, y))

    for i in range(1, X):
        tell(hello_column, (z, lax.rem(x + i, X), c, y))

    R = 2 * T
    row_seq = lax.rem(iota((R, 1), 0), T)
    scores = jnp.zeros((R, L), F32)
    limit = jnp.zeros((R, 1), jnp.int32)
    for b in range(T):
        kv_copies[b].wait()
        scores = jnp.where(row_seq == b, nt(both, kv[b]), scores)
        limit = jnp.where(row_seq == b, lengths_ref[b], limit)
    bias = jnp.where(iota((R, 1), 0) < T, bias_ref[0], bias_ref[1])
    scores = scores * HD ** (-0.5) + bias
    tail = jnp.log1p(jnp.exp(-jnp.abs(scores)))
    visible = iota((R, L), 1) < limit
    survive = jnp.where(visible, jnp.minimum(-scores, 0.0) - tail, 0.0)
    taken = jnp.minimum(scores, 0.0) - tail
    blocks = L // 128
    left = jnp.concatenate([survive[:, k * 128 : (k + 1) * 128] for k in range(blocks)], axis=0)
    later = jnp.where(
        (iota((128, 256), 1) >= 128) | (iota((128, 256), 0) > iota((128, 256), 1)), 1.0, 0.0
    ).astype(BF16)
    sums = jnp.zeros((blocks * R, 256), F32)
    for _ in range(3):
        piece = left.astype(BF16)
        sums = sums + nn(piece, later)
        left = left - piece.astype(F32)
    beyond = jnp.zeros((R, 128), F32)
    parts = []
    for k in reversed(range(blocks)):
        here = slice(k * R, (k + 1) * R)
        span = slice(k * 128, (k + 1) * 128)
        parts.append(
            jnp.where(
                visible[:, span], jnp.exp(taken[:, span] + (sums[here, :128] + beyond)), 0.0
            )
        )
        beyond = beyond + sums[here, 128:]
    weights = jnp.concatenate(parts[::-1], axis=1).astype(BF16)
    blended = jnp.zeros((R, 2 * HD), F32)
    for b in range(T):
        blended = jnp.where(row_seq == b, nn(weights, kv[b]), blended)
    wide = iota((R, 2 * HD), 1)
    square = jnp.sum(jnp.where(wide >= HD, blended * blended, 0.0), axis=1, keepdims=True)
    blended = blended * lax.rsqrt(square / HD + 1e-06)
    heads = jnp.where(lane < HD, pltpu.roll(blended[:T], HD, 1), blended[T:])
    loads["head_gain"].wait()
    normed = (heads * head_gain_ref[...]).astype(BF16)
    loads["wo"].wait()
    att[y] = nn(normed, wo[...]).astype(BF16)


    def send(src, dst, k, device):
        pltpu.make_async_remote_copy(
            src_ref=src,
            dst_ref=dst,
            send_sem=send_sem.at[k],
            recv_sem=recv_sem.at[k],
            device_id=device,
            device_id_type=MESH,
        ).start()

    def arrived(ref, k):
        pltpu.make_async_copy(ref, ref, recv_sem.at[k]).wait()

    def left_here(ref, k):
        pltpu.make_async_copy(ref, ref, send_sem.at[k]).wait()

    for j in range(1, Y):
        send(att.at[y], att.at[y], 0, (z, x, c, lax.rem(y + j, Y)))
    for name in ("dg", "du", "dd"):
        loads[name].wait()
    FD = dg_in.shape[0]
    FDP = dw.shape[1]

    def padded(values):
        spare = jnp.zeros((FDP - FD, values.shape[1]), F32)
        return jnp.concatenate([values.astype(F32), spare], axis=0).astype(BF16)

    dw[xc, :, :D] = padded(dg_in[...])
    dw[xc, :, D : 2 * D] = padded(du_in[...])
    dw[xc, :, 2 * D :] = padded(dd_in[...])
    for i in range(1, X):
        send(dw.at[xc], dw.at[xc], 4, (z, lax.rem(x + i, X), c, y))
    for name in ("eg", "eu", "ed"):
        loads[name].wait()

    @pl.when(c == 0)
    def _():
        pl.semaphore_wait(hello_core, X)

    send(wg.at[c], wg.at[c], 1, sib)
    send(wu.at[c], wu.at[c], 2, sib)
    send(wd.at[c], wd.at[c], 3, sib)
    for i in range(X):
        send(dw.at[xc], dw.at[xc], 4, (z, lax.rem(x + i, X), other, y))

    for name in ("attn_gain", "router", "routes", "mix", "ffn_gain"):
        loads[name].wait()
    token_row = iota((T, 1), 0)
    routes = []
    for j in range(2):
        column = jnp.zeros((T, 1), jnp.int32)
        for t in range(T):
            column = jnp.where(token_row == t, routes_ref[j, t], column)
        routes.append(column)
    experts = router.shape[0]
    lanes = iota((T, 128), 1)
    lane_expert = lax.rem(lanes, experts)
    lane_group = lanes // experts
    hits = [lane_expert == r for r in routes]
    named = jnp.where(hits[0] | hits[1], 1.0, 0.0)
    before = jnp.zeros((T, 128), F32)
    for t in range(T - 1):
        before = before + jnp.where(token_row > t, named[t : t + 1, :], 0.0)
    lane_slot = lax.rem(lane_group, 2).astype(F32)
    placed = jnp.where(before == lane_slot, named, 0.0)
    mix_row = jnp.concatenate(
        [mix_ref[k : k + 1, :].astype(F32) for k in range(D // 128)], axis=1
    )
    arrived(att.at[pl.ds(0, Y - 1)], 0)
    attended = att[0].astype(F32)
    for j in range(1, Y):
        attended = attended + att[j].astype(F32)
    gain = jnp.concatenate([attn_gain_ref[k : k + 1, :] for k in range(D // 128)], axis=1)
    values = RESIDUAL_SCALE * tokens.astype(F32) + attended
    centred = values - jnp.mean(values, axis=1, keepdims=True)
    spread = jnp.mean(centred * centred, axis=1, keepdims=True)
    settled = (centred * lax.rsqrt(spread + 1e-05) * gain).astype(BF16)
    for j in range(Y):
        settled_cols[j] = settled[:, j * DY : (j + 1) * DY]
    logits = nt(settled, router[...])
    mix = 1.0 / (
        1.0 + jnp.exp(-jnp.sum(settled.astype(F32) * mix_row, axis=1, keepdims=True))
    )
    small = iota((T, experts), 1)
    picked = [
        jnp.sum(jnp.where(small == r, logits, 0.0), axis=1, keepdims=True) for r in routes
    ]
    share = [1.0 / (1.0 + jnp.exp(picked[1 - j] - picked[j])) for j in range(2)]
    placed_share = placed * jnp.where(hits[0], share[0], share[1])

    def high(v):
        return v.astype(BF16).astype(F32)

    share_high = high(placed_share)
    mix_high = high(mix)
    table = jnp.where(
        lane_group < 2, placed, jnp.where(lane_group < 4, share_high, placed_share - share_high)
    )
    table = jnp.where(
        lanes < 6 * experts,
        table,
        jnp.where(
            lanes == 6 * experts,
            mix_high,
            jnp.where(lanes == 6 * experts + 1, mix - mix_high, 0.0),
        ),
    )
    rows[y, z, :, DY:] = table.astype(BF16)
    rows[y, z, :, :DY] = settled_cols[y]

    def send_rows(k, _):
        send(rows.at[y, z], rows.at[y, z], 16 + z // (Z // CHUNKS), (k, x, c, y))
        return 0

    def send_rows_later(k, _):
        pl.semaphore_wait(hello_line.at[k], 1)
        return send_rows(k, 0)

    lax.fori_loop(0, z, send_rows, 0)
    lax.fori_loop(z + 1, Z, send_rows_later, 0)
    pl.semaphore_wait(hello_column, X - 1)

    ZC = Z // CHUNKS
    TC = ZC * T
    SC = ZC * CAP
    seat = y * X + x
    sel_row = iota((SC, 128), 0)
    sel_pick = jnp.where(
        iota((SC, 128), 1) == lax.rem(sel_row, CAP) * experts + z, 1.0, 0.0
    ).astype(BF16)
    sel_mask = iota((SC, TC), 0) // CAP == iota((SC, TC), 1) // T
    share_row = iota((3 * SC, 128), 0)
    share_group = jnp.where(share_row < 2 * SC, 2, 4) + lax.rem(share_row, CAP)
    share_pick = jnp.where(
        iota((3 * SC, 128), 1) == share_group * experts + z, 1.0, 0.0
    ).astype(BF16)
    share_mask = iota((TC, 3 * SC), 0) // T == lax.rem(iota((TC, 3 * SC), 1), SC) // CAP
    fact_lane = iota((TC, 128), 1)
    mix_lanes = (fact_lane == 6 * experts) | (fact_lane == 6 * experts + 1)
    F = 2 * wg.shape[1]
    mixing = {}

    def arrived_line(buf, g, k):
        first = g * ZC

        @pl.when(z // ZC == g)
        def _():
            if ZC > 1:
                arrived(buf.at[pl.ds(first, ZC - 1)], k)

        @pl.when(z // ZC != g)
        def _():
            arrived(buf.at[pl.ds(first, ZC)], k)

    def gather(g):
        first = g * ZC
        arrived_line(rows.at[y], g, 16 + g)
        facts = rows[y, first : first + ZC, :, DY:].astype(F32).reshape(TC, 128).astype(BF16)
        select = jnp.where(sel_mask, nt(sel_pick, facts), 0.0).astype(BF16)
        own = rows[y, first : first + ZC, :, :DY].astype(F32).reshape(TC, DY).astype(BF16)
        xe[g, seat] = nn(select, own).astype(BF16)
        for i, j in plane:
            px, py = plane_peer(i, j)
            send(xe.at[g, seat], xe.at[g, seat], 24 + g, (z, px, c, py))
        shares = jnp.where(share_mask, nt(facts, share_pick), 0.0).astype(BF16)
        mixes = jnp.sum(
            jnp.where(mix_lanes, facts.astype(F32), 0.0), axis=1, keepdims=True
        )
        mixing[g] = (shares, mixes)

    def expert(g):
        arrived(xe.at[g, pl.ds(0, X * Y - 1)], 24 + g)
        received = jnp.concatenate(
            [
                xe[g, j * X : (j + 1) * X].astype(F32).reshape(X * SC, DY).astype(BF16)
                for j in range(Y)
            ],
            axis=1,
        )
        gate_pre = nt(received, wg[...].reshape(F, D))
        up_pre = nt(received, wu[...].reshape(F, D))
        hidden = (gate_pre / (1.0 + jnp.exp(-gate_pre)) * up_pre).astype(BF16)
        partial = nn(hidden, wd[...].reshape(F, D))
        for i in range(X):
            for j in range(Y):
                pb[g, j * X + i] = partial[
                    i * SC : (i + 1) * SC, j * DY : (j + 1) * DY
                ].astype(BF16)
        for i, j in plane:
            px, py = plane_peer(i, j)
            send(pb.at[g, py * X + px], pr.at[g, seat], 32 + g, (z, px, c, py))
        pr[g, seat] = pb[g, seat]

    def stacked(a, b):
        return jnp.concatenate([dw[k, :, a:b] for k in range(XC)], axis=0)

    def dense_part(g):
        first = g * ZC
        arrived(rows.at[pl.ds(0, Y - 1), pl.ds(first, ZC), :, pl.ds(0, DY)], 28 + g)
        line = jnp.concatenate(
            [
                rows[j, first : first + ZC, :, :DY].astype(F32).reshape(TC, DY).astype(BF16)
                for j in range(Y)
            ],
            axis=1,
        )
        dense_gate = nt(line, stacked(0, D))
        dense_up = nt(line, stacked(D, 2 * D))
        dense_hidden = (dense_gate / (1.0 + jnp.exp(-dense_gate)) * dense_up).astype(BF16)
        shares, mixes = mixing[g]
        mixing[g] = (shares, nn(dense_hidden, stacked(2 * D, 2 * D + DY)) * mixes)

    def home(g):
        first = g * ZC
        arrived(pr.at[g, pl.ds(0, X * Y - 1)], 32 + g)
        served = jnp.zeros((SC, DY), F32)
        for k in range(X * Y):
            served = served + pr[g, k].astype(F32)
        served_high = served.astype(BF16)
        served_low = (served - served_high.astype(F32)).astype(BF16)
        stack = jnp.concatenate([served_high, served_low, served_high], axis=0)
        shares, dense = mixing[g]
        mixed = dense + nn(shares, stack)
        fb[first : first + ZC] = mixed.reshape(ZC, T, DY).astype(BF16)
        for to in range(first, first + ZC):

            @pl.when(z != to)
            def _(to=to):
                send(fb.at[to], fr.at[z], 10, (to, x, c, y))

            @pl.when(z == to)
            def _(to=to):
                fr[to] = fb[to]

    for g in range(CHUNKS):
        gather(g)
    for g in range(CHUNKS):
        for j in range(1, Y):
            block = rows.at[y, pl.ds(g * ZC, ZC), :, pl.ds(0, DY)]
            send(block, block, 28 + g, (z, x, c, lax.rem(y + j, Y)))
    arrived(wg.at[0], 1)
    arrived(wu.at[0], 2)
    arrived(wd.at[0], 3)
    for g in range(CHUNKS):
        expert(g)
    arrived(dw.at[pl.ds(0, XC - 1)], 4)
    for g in range(CHUNKS):
        dense_part(g)
    for g in range(CHUNKS):
        home(g)

    arrived(fr.at[pl.ds(0, Z - 1)], 10)
    combined = RESIDUAL_SCALE * settled_cols[y].astype(F32)
    combined = combined + jnp.sum(fr[...].astype(F32), axis=0)
    centre = jnp.sum(combined, axis=1, keepdims=True) / DY
    centred = combined - centre
    scatter = jnp.sum(centred * centred, axis=1, keepdims=True)
    stats[y] = jnp.where(lanes == 0, centre, jnp.where(lanes == 1, scatter, 0.0))
    for j in range(1, Y):
        send(stats.at[y], stats.at[y], 11, (z, x, c, lax.rem(y + j, Y)))
    ffn_gain = jnp.concatenate(
        [ffn_gain_ref[k : k + 1, :] for k in range(DY // 128)], axis=1
    )
    arrived(stats.at[pl.ds(0, Y - 1)], 11)
    every = [stats[j] for j in range(Y)]
    mean = sum(e[:, 0:1] for e in every) / Y
    var = sum(e[:, 1:2] + DY * (e[:, 0:1] - mean) * (e[:, 0:1] - mean) for e in every) / D
    out_ref[...] = ((combined - mean) * lax.rsqrt(var + 1e-05) * ffn_gain).astype(BF16)

    put = pltpu.make_async_copy(out_ref, out_hbm, load_sem.at[20])
    put.start()

    left_here(att.at[pl.ds(0, Y - 1)], 0)
    left_here(wg.at[0], 1)
    left_here(wu.at[0], 2)
    left_here(wd.at[0], 3)
    left_here(dw.at[pl.ds(0, XC - 1)], 4)
    left_here(rows.at[y, pl.ds(0, Z - 1)], 16 + z // ZC)
    for g in range(CHUNKS):
        left_here(xe.at[g, pl.ds(0, X * Y - 1)], 24 + g)
        left_here(rows.at[pl.ds(0, Y - 1), pl.ds(g * ZC, ZC), :, pl.ds(0, DY)], 28 + g)
        left_here(pb.at[g, pl.ds(0, X * Y - 1)], 32 + g)
    left_here(fb.at[pl.ds(0, Z - 1)], 10)
    left_here(stats.at[pl.ds(0, Y - 1)], 11)
    put_kv.wait()
    put.wait()


def hand_over(result_in, kv_in, result_out, kv_out, sem):
    copies = [
        pltpu.make_async_copy(result_in, result_out, sem.at[0]),
        pltpu.make_async_copy(kv_in, kv_out, sem.at[1]),
    ]
    for copy in copies:
        copy.start()
    for copy in copies:
        copy.wait()


def body(
    dims,
    tokens,
    kv_cache,
    lengths,
    w_query,
    w_key,
    w_value,
    break_bias,
    head_gain,
    w_output,
    attn_norm_gain,
    w_router,
    routes,
    expert_gate,
    expert_up,
    expert_down,
    dense_gate,
    dense_up,
    dense_down,
    mix_gate,
    ffn_norm_gain,
):
    Z, X, C, Y = dims
    T, D = tokens.shape
    DY = D // Y
    L, HD2 = kv_cache.shape[2:]
    F = expert_gate.shape[1]
    FD = dense_gate.shape[1]
    FDP = -(-FD // 8) * 8
    ZS = Z * CAP
    experts = w_router.shape[1]
    anywhere = pl.BlockSpec(memory_space=pl.ANY)
    V = pltpu.VMEM
    result, new_kv = pl.pallas_call(
        functools.partial(layer_kernel, dims),
        out_shape=(
            jax.ShapeDtypeStruct((T, DY), BF16),
            jax.ShapeDtypeStruct((T, HD2), BF16),
        ),
        in_specs=[anywhere] * 20,
        out_specs=(anywhere, anywhere),
        scratch_shapes=[
            V((T, D), BF16),
            V((T, L, HD2), BF16),
            V((D, HD2), BF16),
            V((2, HD2 // 2, D), BF16),
            V((HD2, D), BF16),
            V((experts, D), BF16),
            V((C, F, D), BF16),
            V((C, F, D), BF16),
            V((C, F, D), BF16),
            V((FD, D), BF16),
            V((FD, D), BF16),
            V((FD, DY), BF16),
            V((X * C, FDP, 2 * D + DY), BF16),
            V((Y, T, D), BF16),
            V((Y, T, DY), BF16),
            V((Y, Z, T, DY + 128), BF16),
            V((CHUNKS, X * Y, ZS // CHUNKS, DY), BF16),
            V((CHUNKS, X * Y, ZS // CHUNKS, DY), BF16),
            V((CHUNKS, X * Y, ZS // CHUNKS, DY), BF16),
            V((Z, T, DY), BF16),
            V((Z, T, DY), BF16),
            V((Y, T, 128), F32),
            pltpu.SMEM((T,), jnp.int32),
            pltpu.SMEM((2,), F32),
            pltpu.SMEM((2, T), jnp.int32),
            V((1, HD2), F32),
            V((D // 128, 128), F32),
            V((D // 128, 128), BF16),
            V((DY // 128, 128), F32),
            V((T, DY), BF16),
            V((T, HD2), BF16),
            pltpu.SemaphoreType.DMA((21,)),
            pltpu.SemaphoreType.DMA((T,)),
            pltpu.SemaphoreType.DMA((36,)),
            pltpu.SemaphoreType.DMA((36,)),
            pltpu.SemaphoreType.REGULAR((dims[0],)),
            pltpu.SemaphoreType.REGULAR,
            pltpu.SemaphoreType.REGULAR,
        ],
        compiler_params=pltpu.CompilerParams(
            collective_id=0, has_side_effects=True, vmem_limit_bytes=67043328
        ),
        name="layer",
    )(
        tokens,
        kv_cache.reshape(T, L, HD2),
        lengths,
        w_query,
        w_key.T,
        w_value.T,
        break_bias,
        head_gain.reshape(1, HD2),
        w_output,
        attn_norm_gain.reshape(D // 128, 128),
        w_router.T,
        routes.T,
        expert_gate.T,
        expert_up.T,
        expert_down,
        dense_gate.T,
        dense_up.T,
        dense_down,
        mix_gate.reshape(D // 128, 128),
        ffn_norm_gain.reshape(DY // 128, 128),
    )
    result, new_kv = pl.pallas_call(
        hand_over,
        out_shape=(
            jax.ShapeDtypeStruct((T, DY), BF16),
            jax.ShapeDtypeStruct((T, HD2), BF16),
        ),
        in_specs=[anywhere] * 2,
        out_specs=(anywhere, anywhere),
        scratch_shapes=[pltpu.SemaphoreType.DMA((2,))],
        name="hand_over",
    )(result, new_kv)
    return result, new_kv.reshape(T, 1, HD2)


def solution(mesh):
    cores = 2
    ep, tp = mesh.shape["ep"], mesh.shape["tp"]
    dims = (ep // (4 * cores), 4, cores, tp)
    split = Mesh(mesh.devices.reshape(dims), EP_TP)
    return jax.shard_map(
        functools.partial(body, dims),
        mesh=split,
        in_specs=(
            P(EP, None),
            P(EP, "tp", None, None),
            P(EP),
            P(None, "tp"),
            P(None, "tp"),
            P(None, "tp"),
            P("tp"),
            P("tp"),
            P("tp", None),
            P(),
            P(),
            P(EP, None),
            P(None, EP_TP),
            P(None, EP_TP),
            P(EP_TP, None),
            P(None, EP),
            P(None, EP),
            P(EP, "tp"),
            P(),
            P("tp"),
        ),
        out_specs=(P(EP, "tp"), P(EP, "tp", None)),
        check_vma=False,
    )
```

time: 57.9 us -> 52.3 us (0.903)
  the two profiles are of different devices: /device:TPU:32 before, /device:TPU:6 now
where the time goes in v2:
time: 52.3 us; the launch traced here: 52.1 us
  Pallas kernels  51.5 us (98%)
  between operations  0.65 us (1%)
    pallas_call x1, Pallas kernels, body(): pl.pallas_call(functools.partial(layer_kernel, dims), out_shape=(jax.Shap...  50.2 us
    pallas_call x1, Pallas kernels, body(): pl.pallas_call(hand_over, out_shape=(jax.ShapeDtypeStruct((T, DY), BF16),...  1.31 us

profile of v2, /device:TPU:6, one launch (start us, length us, event | category | flops | bytes accessed | tf_op | source)
XLA Modules:
  0.0 52.1 jit_solution(5045844157037327827)
XLA Ops:
  0.6 50.2 %layer.1 = (bf16[8,256]{1,0:T(8,128)(2,1)}, bf16[8,128]{1,0:T(8,128)(2,1)}) custom-call(bf16[8,1024]{1,0:T(8,128)(2,1)} %tokens_hbm.1, bf16[8,1024,128]{2,1,0:T(8,128)(2,1)} %bitcast.14, s32[8]{0:T(128)} %lengths_hbm.1, bf16[1024,128]{1,0:T(8,128)(2,1)} %wq_hbm.1, bf16[64,1024]{1,0:T(8,128)(2,1)} %bitcast.17, bf16[64,1024]{1,0:T(8,128)(2,1)} %bitcast.18, ...), custom_call_target="tpu_custom_call" | custom-call | tf_op jit(solution)/shard_map/layer/pallas_call | solution.py:578
  50.8 1.3 %hand_over.1 = (bf16[8,256]{1,0:T(8,128)(2,1)}, bf16[8,128]{1,0:T(8,128)(2,1)}) custom-call(bf16[8,256]{1,0:T(8,128)(2,1)} %get-tuple-element.6.result_in, bf16[8,128]{1,0:T(8,128)(2,1)} %get-tuple-element.7.kv_in), custom_call_target="tpu_custom_call" | custom-call | tf_op jit(solution)/shard_map/hand_over/pallas_call | solution.py:652

commit v3 on v2

--- a/solution.py
+++ b/solution.py
@@ -52,8 +52,8 @@
     dd_hbm,
     mix_hbm,
     ffn_gain_hbm,
-    out_hbm,
-    new_kv_hbm,
+    out_ref,
+    new_kv_ref,
     tok,
     kv,
     wq,
@@ -83,8 +83,6 @@
     attn_gain_ref,
     mix_ref,
     ffn_gain_ref,
-    out_ref,
-    new_kv_ref,
     load_sem,
     kv_sem,
     send_sem,
@@ -92,6 +90,8 @@
     hello_line,
     hello_core,
     hello_column,
+    hello_x,
+    hello_y,
 ):
     Z, X, C, Y = dims
     z, x, c, y = (lax.axis_index(a) for a in EP_TP)
@@ -138,10 +138,10 @@
     def tell(sem, device):
         pl.semaphore_signal(sem, inc=1, device_id=device, device_id_type=MESH)
 
-    for j in range(1, Y):
-        tell(barrier, (z, x, c, lax.rem(y + j, Y)))
-    for i in range(1, X):
-        tell(barrier, (z, lax.rem(x + i, X), c, y))
+    y_near = [(z, x, c, lax.rem(y + j, Y)) for j in sorted({1, Y - 1} - {0})]
+    x_near = [(z, lax.rem(x + i, X), c, y) for i in sorted({1, X - 1} - {0})]
+    for device in y_near + x_near:
+        tell(barrier, device)
 
     def tell_later(k, _):
         tell(barrier, (k, x, c, y))
@@ -151,8 +151,7 @@
 
     @pl.when(c == 0)
     def _():
-        for i in range(X):
-            tell(barrier, (z, lax.rem(x + i, X), other, y))
+        tell(barrier, sib)
 
     plane = [(i, j) for i in range(X) for j in range(Y) if (i, j) != (0, 0)]
     plane.sort(key=lambda p: -(min(p[0], X - p[0]) + min(p[1], Y - p[1])))
@@ -172,12 +171,10 @@
     loads["wk"].wait()
     loads["wv"].wait()
     new_kv_ref[...] = nt(tokens, wkv[...].reshape(2 * HD, D)).astype(BF16)
-    put_kv = pltpu.make_async_copy(new_kv_ref, new_kv_hbm, load_sem.at[19])
-    put_kv.start()
 
     loads["lengths"].wait()
     loads["bias"].wait()
-    pl.semaphore_wait(barrier, Y - 1 + X - 1 + z + c * X)
+    pl.semaphore_wait(barrier, len(y_near) + len(x_near) + z + c)
 
     def answer(k, _):
         tell(hello_line.at[z], (k, x, c, y))
@@ -187,11 +184,12 @@
 
     @pl.when(c == 1)
     def _():
-        for i in range(X):
-            tell(hello_core, (z, lax.rem(x + i, X), other, y))
-
-    for i in range(1, X):
-        tell(hello_column, (z, lax.rem(x + i, X), c, y))
+        tell(hello_core, sib)
+
+    for device in y_near:
+        tell(hello_y, device)
+    for device in x_near:
+        tell(hello_x, device)
 
     R = 2 * T
     row_seq = lax.rem(iota((R, 1), 0), T)
@@ -258,8 +256,12 @@
     def left_here(ref, k):
         pltpu.make_async_copy(ref, ref, send_sem.at[k]).wait()
 
+    pl.semaphore_wait(hello_y, len(y_near))
     for j in range(1, Y):
         send(att.at[y], att.at[y], 0, (z, x, c, lax.rem(y + j, Y)))
+    pl.semaphore_wait(hello_x, len(x_near))
+    for i in range(1, X):
+        tell(hello_column, (z, lax.rem(x + i, X), c, y))
     for name in ("dg", "du", "dd"):
         loads[name].wait()
     FD = dg_in.shape[0]
@@ -279,13 +281,12 @@
 
     @pl.when(c == 0)
     def _():
-        pl.semaphore_wait(hello_core, X)
+        pl.semaphore_wait(hello_core, 1)
 
     send(wg.at[c], wg.at[c], 1, sib)
     send(wu.at[c], wu.at[c], 2, sib)
     send(wd.at[c], wd.at[c], 3, sib)
-    for i in range(X):
-        send(dw.at[xc], dw.at[xc], 4, (z, lax.rem(x + i, X), other, y))
+    send(dw.at[xc], dw.at[xc], 5, sib)
 
     for name in ("attn_gain", "router", "routes", "mix", "ffn_gain"):
         loads[name].wait()
@@ -363,6 +364,10 @@
     lax.fori_loop(0, z, send_rows, 0)
     lax.fori_loop(z + 1, Z, send_rows_later, 0)
     pl.semaphore_wait(hello_column, X - 1)
+    arrived(dw.at[pl.ds(0, X - 1)], 4)
+    for i in range(1, X):
+        passed = lax.rem(x + i, X) * C + c
+        send(dw.at[passed], dw.at[passed], 5, sib)
 
     ZC = Z // CHUNKS
     TC = ZC * T
@@ -476,22 +481,25 @@
             def _(to=to):
                 fr[to] = fb[to]
 
-    for g in range(CHUNKS):
-        gather(g)
-    for g in range(CHUNKS):
+    def spread_tokens(g):
         for j in range(1, Y):
             block = rows.at[y, pl.ds(g * ZC, ZC), :, pl.ds(0, DY)]
             send(block, block, 28 + g, (z, x, c, lax.rem(y + j, Y)))
+
+    gather(0)
+    gather(1)
+    spread_tokens(0)
     arrived(wg.at[0], 1)
     arrived(wu.at[0], 2)
     arrived(wd.at[0], 3)
-    for g in range(CHUNKS):
-        expert(g)
-    arrived(dw.at[pl.ds(0, XC - 1)], 4)
-    for g in range(CHUNKS):
-        dense_part(g)
-    for g in range(CHUNKS):
-        home(g)
+    expert(0)
+    expert(1)
+    spread_tokens(1)
+    arrived(dw.at[pl.ds(0, X)], 5)
+    dense_part(0)
+    home(0)
+    dense_part(1)
+    home(1)
 
     arrived(fr.at[pl.ds(0, Z - 1)], 10)
     combined = RESIDUAL_SCALE * settled_cols[y].astype(F32)
@@ -511,14 +519,12 @@
     var = sum(e[:, 1:2] + DY * (e[:, 0:1] - mean) * (e[:, 0:1] - mean) for e in every) / D
     out_ref[...] = ((combined - mean) * lax.rsqrt(var + 1e-05) * ffn_gain).astype(BF16)
 
-    put = pltpu.make_async_copy(out_ref, out_hbm, load_sem.at[20])
-    put.start()
-
     left_here(att.at[pl.ds(0, Y - 1)], 0)
     left_here(wg.at[0], 1)
     left_here(wu.at[0], 2)
     left_here(wd.at[0], 3)
-    left_here(dw.at[pl.ds(0, XC - 1)], 4)
+    left_here(dw.at[pl.ds(0, X - 1)], 4)
+    left_here(dw.at[pl.ds(0, X)], 5)
     left_here(rows.at[y, pl.ds(0, Z - 1)], 16 + z // ZC)
     for g in range(CHUNKS):
         left_here(xe.at[g, pl.ds(0, X * Y - 1)], 24 + g)
@@ -526,8 +532,6 @@
         left_here(pb.at[g, pl.ds(0, X * Y - 1)], 32 + g)
     left_here(fb.at[pl.ds(0, Z - 1)], 10)
     left_here(stats.at[pl.ds(0, Y - 1)], 11)
-    put_kv.wait()
-    put.wait()
 
 
 def hand_over(result_in, kv_in, result_out, kv_out, sem):
@@ -582,7 +586,7 @@
             jax.ShapeDtypeStruct((T, HD2), BF16),
         ),
         in_specs=[anywhere] * 20,
-        out_specs=(anywhere, anywhere),
+        out_specs=(pl.BlockSpec(memory_space=pltpu.VMEM),) * 2,
         scratch_shapes=[
             V((T, D), BF16),
             V((T, L, HD2), BF16),
@@ -613,13 +617,13 @@
             V((D // 128, 128), F32),
             V((D // 128, 128), BF16),
             V((DY // 128, 128), F32),
-            V((T, DY), BF16),
-            V((T, HD2), BF16),
-            pltpu.SemaphoreType.DMA((21,)),
+            pltpu.SemaphoreType.DMA((19,)),
             pltpu.SemaphoreType.DMA((T,)),
             pltpu.SemaphoreType.DMA((36,)),
             pltpu.SemaphoreType.DMA((36,)),
             pltpu.SemaphoreType.REGULAR((dims[0],)),
+            pltpu.SemaphoreType.REGULAR,
+            pltpu.SemaphoreType.REGULAR,
             pltpu.SemaphoreType.REGULAR,
             pltpu.SemaphoreType.REGULAR,
         ],

time: 52.3 us -> 50.6 us (0.967)
  Pallas kernels: 51.5 us -> 49.8 us
    pallas_call x1, Pallas kernels: 50.2 us -> 48.5 us  [body(): pl.pallas_call(functools.partial(layer_kernel, dims), out_shape=(jax.Shap...]
where the time goes in v3:
time: 50.6 us; the launch traced here: 50.5 us
  Pallas kernels  49.8 us (98%)
  between operations  0.65 us (1%)
    pallas_call x1, Pallas kernels, body(): pl.pallas_call(functools.partial(layer_kernel, dims), out_shape=(jax.Shap...  48.5 us
    pallas_call x1, Pallas kernels, body(): pl.pallas_call(hand_over, out_shape=(jax.ShapeDtypeStruct((T, DY), BF16),...  1.31 us

profile of v3, /device:TPU:6, one launch (start us, length us, event | category | flops | bytes accessed | tf_op | source)
XLA Modules:
  0.0 50.5 jit_solution(15165201333374239093)
XLA Ops:
  0.6 48.5 %layer.1 = (bf16[8,256]{1,0:T(8,128)(2,1)}, bf16[8,128]{1,0:T(8,128)(2,1)}) custom-call(bf16[8,1024]{1,0:T(8,128)(2,1)} %tokens_hbm.1, bf16[8,1024,128]{2,1,0:T(8,128)(2,1)} %bitcast.14, s32[8]{0:T(128)} %lengths_hbm.1, bf16[1024,128]{1,0:T(8,128)(2,1)} %wq_hbm.1, bf16[64,1024]{1,0:T(8,128)(2,1)} %bitcast.17, bf16[64,1024]{1,0:T(8,128)(2,1)} %bitcast.18, ...), custom_call_target="tpu_custom_call" | custom-call | tf_op jit(solution)/shard_map/layer/pallas_call | solution.py:582
  49.2 1.3 %hand_over.1 = (bf16[8,256]{1,0:T(8,128)(2,1)}, bf16[8,128]{1,0:T(8,128)(2,1)}) custom-call(bf16[8,256]{1,0:T(8,128)(2,1)} %get-tuple-element.6.result_in, bf16[8,128]{1,0:T(8,128)(2,1)} %get-tuple-element.7.kv_in), custom_call_target="tpu_custom_call" | custom-call | tf_op jit(solution)/shard_map/hand_over/pallas_call | solution.py:656

commit v4 on v3

--- a/solution.py
+++ b/solution.py
@@ -354,7 +354,7 @@
     rows[y, z, :, :DY] = settled_cols[y]
 
     def send_rows(k, _):
-        send(rows.at[y, z], rows.at[y, z], 16 + z // (Z // CHUNKS), (k, x, c, y))
+        send(rows.at[y, z], rows.at[y, z], 8 + z // (Z // CHUNKS), (k, x, c, y))
         return 0
 
     def send_rows_later(k, _):
@@ -403,14 +403,14 @@
 
     def gather(g):
         first = g * ZC
-        arrived_line(rows.at[y], g, 16 + g)
+        arrived_line(rows.at[y], g, 8 + g)
         facts = rows[y, first : first + ZC, :, DY:].astype(F32).reshape(TC, 128).astype(BF16)
         select = jnp.where(sel_mask, nt(sel_pick, facts), 0.0).astype(BF16)
         own = rows[y, first : first + ZC, :, :DY].astype(F32).reshape(TC, DY).astype(BF16)
         xe[g, seat] = nn(select, own).astype(BF16)
         for i, j in plane:
             px, py = plane_peer(i, j)
-            send(xe.at[g, seat], xe.at[g, seat], 24 + g, (z, px, c, py))
+            send(xe.at[g, seat], xe.at[g, seat], 10 + g, (z, px, c, py))
         shares = jnp.where(share_mask, nt(facts, share_pick), 0.0).astype(BF16)
         mixes = jnp.sum(
             jnp.where(mix_lanes, facts.astype(F32), 0.0), axis=1, keepdims=True
@@ -418,10 +418,10 @@
         mixing[g] = (shares, mixes)
 
     def expert(g):
-        arrived(xe.at[g, pl.ds(0, X * Y - 1)], 24 + g)
+        arrived(xe.at[g, pl.ds(0, X * Y - 1)], 10 + g)
         received = jnp.concatenate(
             [
-                xe[g, j * X : (j + 1) * X].astype(F32).reshape(X * SC, DY).astype(BF16)
+                xe[g, j * X : (j + 1) * X].reshape(X * SC, DY)
                 for j in range(Y)
             ],
             axis=1,
@@ -437,7 +437,7 @@
                 ].astype(BF16)
         for i, j in plane:
             px, py = plane_peer(i, j)
-            send(pb.at[g, py * X + px], pr.at[g, seat], 32 + g, (z, px, c, py))
+            send(pb.at[g, py * X + px], pr.at[g, seat], 14 + g, (z, px, c, py))
         pr[g, seat] = pb[g, seat]
 
     def stacked(a, b):
@@ -445,7 +445,7 @@
 
     def dense_part(g):
         first = g * ZC
-        arrived(rows.at[pl.ds(0, Y - 1), pl.ds(first, ZC), :, pl.ds(0, DY)], 28 + g)
+        arrived(rows.at[pl.ds(0, Y - 1), pl.ds(first, ZC), :, pl.ds(0, DY)], 12 + g)
         line = jnp.concatenate(
             [
                 rows[j, first : first + ZC, :, :DY].astype(F32).reshape(TC, DY).astype(BF16)
@@ -461,7 +461,7 @@
 
     def home(g):
         first = g * ZC
-        arrived(pr.at[g, pl.ds(0, X * Y - 1)], 32 + g)
+        arrived(pr.at[g, pl.ds(0, X * Y - 1)], 14 + g)
         served = jnp.zeros((SC, DY), F32)
         for k in range(X * Y):
             served = served + pr[g, k].astype(F32)
@@ -475,7 +475,7 @@
 
             @pl.when(z != to)
             def _(to=to):
-                send(fb.at[to], fr.at[z], 10, (to, x, c, y))
+                send(fb.at[to], fr.at[z], 6, (to, x, c, y))
 
             @pl.when(z == to)
             def _(to=to):
@@ -484,7 +484,7 @@
     def spread_tokens(g):
         for j in range(1, Y):
             block = rows.at[y, pl.ds(g * ZC, ZC), :, pl.ds(0, DY)]
-            send(block, block, 28 + g, (z, x, c, lax.rem(y + j, Y)))
+            send(block, block, 12 + g, (z, x, c, lax.rem(y + j, Y)))
 
     gather(0)
     gather(1)
@@ -501,7 +501,7 @@
     dense_part(1)
     home(1)
 
-    arrived(fr.at[pl.ds(0, Z - 1)], 10)
+    arrived(fr.at[pl.ds(0, Z - 1)], 6)
     combined = RESIDUAL_SCALE * settled_cols[y].astype(F32)
     combined = combined + jnp.sum(fr[...].astype(F32), axis=0)
     centre = jnp.sum(combined, axis=1, keepdims=True) / DY
@@ -509,11 +509,11 @@
     scatter = jnp.sum(centred * centred, axis=1, keepdims=True)
     stats[y] = jnp.where(lanes == 0, centre, jnp.where(lanes == 1, scatter, 0.0))
     for j in range(1, Y):
-        send(stats.at[y], stats.at[y], 11, (z, x, c, lax.rem(y + j, Y)))
+        send(stats.at[y], stats.at[y], 7, (z, x, c, lax.rem(y + j, Y)))
     ffn_gain = jnp.concatenate(
         [ffn_gain_ref[k : k + 1, :] for k in range(DY // 128)], axis=1
     )
-    arrived(stats.at[pl.ds(0, Y - 1)], 11)
+    arrived(stats.at[pl.ds(0, Y - 1)], 7)
     every = [stats[j] for j in range(Y)]
     mean = sum(e[:, 0:1] for e in every) / Y
     var = sum(e[:, 1:2] + DY * (e[:, 0:1] - mean) * (e[:, 0:1] - mean) for e in every) / D
@@ -525,13 +525,13 @@
     left_here(wd.at[0], 3)
     left_here(dw.at[pl.ds(0, X - 1)], 4)
     left_here(dw.at[pl.ds(0, X)], 5)
-    left_here(rows.at[y, pl.ds(0, Z - 1)], 16 + z // ZC)
+    left_here(rows.at[y, pl.ds(0, Z - 1)], 8 + z // ZC)
     for g in range(CHUNKS):
-        left_here(xe.at[g, pl.ds(0, X * Y - 1)], 24 + g)
-        left_here(rows.at[pl.ds(0, Y - 1), pl.ds(g * ZC, ZC), :, pl.ds(0, DY)], 28 + g)
-        left_here(pb.at[g, pl.ds(0, X * Y - 1)], 32 + g)
-    left_here(fb.at[pl.ds(0, Z - 1)], 10)
-    left_here(stats.at[pl.ds(0, Y - 1)], 11)
+        left_here(xe.at[g, pl.ds(0, X * Y - 1)], 10 + g)
+        left_here(rows.at[pl.ds(0, Y - 1), pl.ds(g * ZC, ZC), :, pl.ds(0, DY)], 12 + g)
+        left_here(pb.at[g, pl.ds(0, X * Y - 1)], 14 + g)
+    left_here(fb.at[pl.ds(0, Z - 1)], 6)
+    left_here(stats.at[pl.ds(0, Y - 1)], 7)
 
 
 def hand_over(result_in, kv_in, result_out, kv_out, sem):
@@ -581,10 +581,7 @@
     V = pltpu.VMEM
     result, new_kv = pl.pallas_call(
         functools.partial(layer_kernel, dims),
-        out_shape=(
-            jax.ShapeDtypeStruct((T, DY), BF16),
-            jax.ShapeDtypeStruct((T, HD2), BF16),
-        ),
+        out_shape=(V((T, DY), BF16), V((T, HD2), BF16)),
         in_specs=[anywhere] * 20,
         out_specs=(pl.BlockSpec(memory_space=pltpu.VMEM),) * 2,
         scratch_shapes=[
@@ -619,8 +616,8 @@
             V((DY // 128, 128), F32),
             pltpu.SemaphoreType.DMA((19,)),
             pltpu.SemaphoreType.DMA((T,)),
-            pltpu.SemaphoreType.DMA((36,)),
-            pltpu.SemaphoreType.DMA((36,)),
+            pltpu.SemaphoreType.DMA((16,)),
+            pltpu.SemaphoreType.DMA((16,)),
             pltpu.SemaphoreType.REGULAR((dims[0],)),
             pltpu.SemaphoreType.REGULAR,
             pltpu.SemaphoreType.REGULAR,
@@ -628,7 +625,7 @@
             pltpu.SemaphoreType.REGULAR,
         ],
         compiler_params=pltpu.CompilerParams(
-            collective_id=0, has_side_effects=True, vmem_limit_bytes=67043328
+            collective_id=0, has_side_effects=True, vmem_limit_bytes=64000000
         ),
         name="layer",
     )(
@@ -659,9 +656,10 @@
             jax.ShapeDtypeStruct((T, DY), BF16),
             jax.ShapeDtypeStruct((T, HD2), BF16),
         ),
-        in_specs=[anywhere] * 2,
+        in_specs=[pl.BlockSpec(memory_space=pltpu.VMEM)] * 2,
         out_specs=(anywhere, anywhere),
         scratch_shapes=[pltpu.SemaphoreType.DMA((2,))],
+        compiler_params=pltpu.CompilerParams(vmem_limit_bytes=1024 * 1024),
         name="hand_over",
     )(result, new_kv)
     return result, new_kv.reshape(T, 1, HD2)

time: 50.6 us -> 49.2 us (0.972)
  Pallas kernels: 49.8 us -> 48.4 us
    pallas_call x1, Pallas kernels: 48.5 us -> 47.8 us  [body(): pl.pallas_call(functools.partial(layer_kernel, dims), out_shape=(V((T, DY...]
    pallas_call x1, Pallas kernels: 1.31 us -> 0.61 us  [body(): pl.pallas_call(hand_over, out_shape=(jax.ShapeDtypeStruct((T, DY), BF16),...]
where the time goes in v4:
time: 49.2 us; the launch traced here: 49 us
  Pallas kernels  48.4 us (98%)
  between operations  0.65 us (1%)
    pallas_call x1, Pallas kernels, body(): pl.pallas_call(functools.partial(layer_kernel, dims), out_shape=(V((T, DY...  47.8 us

profile of v4, /device:TPU:6, one launch (start us, length us, event | category | flops | bytes accessed | tf_op | source)
XLA Modules:
  0.0 49.0 jit_solution(11312861986109913444)
XLA Ops:
  0.6 47.8 %layer.1 = (bf16[8,256]{1,0:T(8,128)(2,1)S(1)}, bf16[8,128]{1,0:T(8,128)(2,1)S(1)}) custom-call(bf16[8,1024]{1,0:T(8,128)(2,1)} %tokens_hbm.1, bf16[8,1024,128]{2,1,0:T(8,128)(2,1)} %bitcast.14, s32[8]{0:T(128)} %lengths_hbm.1, bf16[1024,128]{1,0:T(8,128)(2,1)} %wq_hbm.1, bf16[64,1024]{1,0:T(8,128)(2,1)} %bitcast.17, bf16[64,1024]{1,0:T(8,128)(2,1)} %bitcast.18, ...), custom_call_target="tpu_custom_call" | custom-call | tf_op jit(solution)/shard_map/layer/pallas_call | solution.py:582
  48.4 0.6 %hand_over.1 = (bf16[8,256]{1,0:T(8,128)(2,1)}, bf16[8,128]{1,0:T(8,128)(2,1)}) custom-call(bf16[8,256]{1,0:T(8,128)(2,1)S(1)} %get-tuple-element.6.result_in, bf16[8,128]{1,0:T(8,128)(2,1)S(1)} %get-tuple-element.7.kv_in), custom_call_target="tpu_custom_call" | custom-call | tf_op jit(solution)/shard_map/hand_over/pallas_call | solution.py:653

commit v5 on v4

--- a/solution.py
+++ b/solution.py
@@ -411,11 +411,6 @@
         for i, j in plane:
             px, py = plane_peer(i, j)
             send(xe.at[g, seat], xe.at[g, seat], 10 + g, (z, px, c, py))
-        shares = jnp.where(share_mask, nt(facts, share_pick), 0.0).astype(BF16)
-        mixes = jnp.sum(
-            jnp.where(mix_lanes, facts.astype(F32), 0.0), axis=1, keepdims=True
-        )
-        mixing[g] = (shares, mixes)
 
     def expert(g):
         arrived(xe.at[g, pl.ds(0, X * Y - 1)], 10 + g)
@@ -456,7 +451,11 @@
         dense_gate = nt(line, stacked(0, D))
         dense_up = nt(line, stacked(D, 2 * D))
         dense_hidden = (dense_gate / (1.0 + jnp.exp(-dense_gate)) * dense_up).astype(BF16)
-        shares, mixes = mixing[g]
+        facts = rows[y, first : first + ZC, :, DY:].astype(F32).reshape(TC, 128).astype(BF16)
+        shares = jnp.where(share_mask, nt(facts, share_pick), 0.0).astype(BF16)
+        mixes = jnp.sum(
+            jnp.where(mix_lanes, facts.astype(F32), 0.0), axis=1, keepdims=True
+        )
         mixing[g] = (shares, nn(dense_hidden, stacked(2 * D, 2 * D + DY)) * mixes)
 
     def home(g):
@@ -486,18 +485,37 @@
             block = rows.at[y, pl.ds(g * ZC, ZC), :, pl.ds(0, DY)]
             send(block, block, 12 + g, (z, x, c, lax.rem(y + j, Y)))
 
+    early = z < Z // 2
     gather(0)
-    gather(1)
+
+    @pl.when(jnp.logical_not(early))
+    def _():
+        gather(1)
+
     spread_tokens(0)
     arrived(wg.at[0], 1)
     arrived(wu.at[0], 2)
     arrived(wd.at[0], 3)
     expert(0)
-    expert(1)
-    spread_tokens(1)
+
+    @pl.when(early)
+    def _():
+        gather(1)
+        spread_tokens(1)
+
+    @pl.when(jnp.logical_not(early))
+    def _():
+        expert(1)
+        spread_tokens(1)
+
     arrived(dw.at[pl.ds(0, X)], 5)
     dense_part(0)
     home(0)
+
+    @pl.when(early)
+    def _():
+        expert(1)
+
     dense_part(1)
     home(1)
 

time: 49.2 us -> 48.5 us (0.986)
  Pallas kernels: 48.4 us -> 47.5 us
    pallas_call x1, Pallas kernels: 47.8 us -> 46.9 us  [body(): pl.pallas_call(functools.partial(layer_kernel, dims), out_shape=(V((T, DY...]
where the time goes in v5:
time: 48.5 us; the launch traced here: 48.1 us
  Pallas kernels  47.5 us (98%)
  between operations  0.65 us (1%)
    pallas_call x1, Pallas kernels, body(): pl.pallas_call(functools.partial(layer_kernel, dims), out_shape=(V((T, DY...  46.9 us

profile of v5, /device:TPU:6, one launch (start us, length us, event | category | flops | bytes accessed | tf_op | source)
XLA Modules:
  0.0 48.1 jit_solution(9599010670102105421)
XLA Ops:
  0.6 46.9 %layer.1 = (bf16[8,256]{1,0:T(8,128)(2,1)S(1)}, bf16[8,128]{1,0:T(8,128)(2,1)S(1)}) custom-call(bf16[8,1024]{1,0:T(8,128)(2,1)} %tokens_hbm.1, bf16[8,1024,128]{2,1,0:T(8,128)(2,1)} %bitcast.14, s32[8]{0:T(128)} %lengths_hbm.1, bf16[1024,128]{1,0:T(8,128)(2,1)} %wq_hbm.1, bf16[64,1024]{1,0:T(8,128)(2,1)} %bitcast.17, bf16[64,1024]{1,0:T(8,128)(2,1)} %bitcast.18, ...), custom_call_target="tpu_custom_call" | custom-call | tf_op jit(solution)/shard_map/layer/pallas_call | solution.py:600
  47.5 0.6 %hand_over.1 = (bf16[8,256]{1,0:T(8,128)(2,1)}, bf16[8,128]{1,0:T(8,128)(2,1)}) custom-call(bf16[8,256]{1,0:T(8,128)(2,1)S(1)} %get-tuple-element.6.result_in, bf16[8,128]{1,0:T(8,128)(2,1)S(1)} %get-tuple-element.7.kv_in), custom_call_target="tpu_custom_call" | custom-call | tf_op jit(solution)/shard_map/hand_over/pallas_call | solution.py:671

commit v6 on v5

--- a/solution.py
+++ b/solution.py
@@ -60,9 +60,7 @@
     wkv,
     wo,
     router,
-    wg,
-    wu,
-    wd,
+    we,
     dg_in,
     du_in,
     dd_in,
@@ -84,7 +82,6 @@
     mix_ref,
     ffn_gain_ref,
     load_sem,
-    kv_sem,
     send_sem,
     recv_sem,
     hello_line,
@@ -112,26 +109,24 @@
 
     load("tok", 0, tokens_hbm, tok)
     load("wq", 1, wq_hbm, wq)
-    load("lengths", 12, lengths_hbm, lengths_ref)
-    load("bias", 13, bias_hbm, bias_ref)
+    load("lengths", 10, lengths_hbm, lengths_ref)
+    load("bias", 11, bias_hbm, bias_ref)
     load("wk", 2, wk_hbm, wkv.at[0])
-    load("wv", 3, wv_hbm, wkv.at[1])
-    kv_copies = [pltpu.make_async_copy(kv_hbm.at[b], kv.at[b], kv_sem.at[b]) for b in range(T)]
-    for copy in kv_copies:
-        copy.start()
+    load("wv", 2, wv_hbm, wkv.at[1])
+    load("kv", 3, kv_hbm, kv)
     load("dg", 4, dg_hbm, dg_in)
     load("du", 5, du_hbm, du_in)
     load("dd", 6, dd_hbm, dd_in)
     load("wo", 7, wo_hbm, wo)
     load("router", 8, router_hbm, router)
-    load("head_gain", 14, head_gain_hbm, head_gain_ref)
-    load("attn_gain", 15, attn_gain_hbm, attn_gain_ref)
-    load("routes", 16, routes_hbm, routes_ref)
-    load("mix", 17, mix_hbm, mix_ref)
-    load("ffn_gain", 18, ffn_gain_hbm, ffn_gain_ref)
-    load("eg", 9, eg_hbm, wg.at[c])
-    load("eu", 10, eu_hbm, wu.at[c])
-    load("ed", 11, ed_hbm, wd.at[c])
+    load("head_gain", 12, head_gain_hbm, head_gain_ref)
+    load("attn_gain", 13, attn_gain_hbm, attn_gain_ref)
+    load("routes", 14, routes_hbm, routes_ref)
+    load("mix", 15, mix_hbm, mix_ref)
+    load("ffn_gain", 16, ffn_gain_hbm, ffn_gain_ref)
+    load("eg", 9, eg_hbm, we.at[c, 0])
+    load("eu", 9, eu_hbm, we.at[c, 1])
+    load("ed", 9, ed_hbm, we.at[c, 2])
 
     barrier = pltpu.get_barrier_semaphore()
 
@@ -168,8 +163,7 @@
     both = jnp.concatenate(
         [jnp.where(lane < HD, queries, 0.0), jnp.where(lane < HD, turned, 0.0)], axis=0
     ).astype(BF16)
-    loads["wk"].wait()
-    loads["wv"].wait()
+    pltpu.make_async_copy(wkv, wkv, load_sem.at[2]).wait()
     new_kv_ref[...] = nt(tokens, wkv[...].reshape(2 * HD, D)).astype(BF16)
 
     loads["lengths"].wait()
@@ -195,8 +189,8 @@
     row_seq = lax.rem(iota((R, 1), 0), T)
     scores = jnp.zeros((R, L), F32)
     limit = jnp.zeros((R, 1), jnp.int32)
+    loads["kv"].wait()
     for b in range(T):
-        kv_copies[b].wait()
         scores = jnp.where(row_seq == b, nt(both, kv[b]), scores)
         limit = jnp.where(row_seq == b, lengths_ref[b], limit)
     bias = jnp.where(iota((R, 1), 0) < T, bias_ref[0], bias_ref[1])
@@ -276,16 +270,13 @@
     dw[xc, :, 2 * D :] = padded(dd_in[...])
     for i in range(1, X):
         send(dw.at[xc], dw.at[xc], 4, (z, lax.rem(x + i, X), c, y))
-    for name in ("eg", "eu", "ed"):
-        loads[name].wait()
+    pltpu.make_async_copy(we.at[c], we.at[c], load_sem.at[9]).wait()
 
     @pl.when(c == 0)
     def _():
         pl.semaphore_wait(hello_core, 1)
 
-    send(wg.at[c], wg.at[c], 1, sib)
-    send(wu.at[c], wu.at[c], 2, sib)
-    send(wd.at[c], wd.at[c], 3, sib)
+    send(we.at[c], we.at[c], 1, sib)
     send(dw.at[xc], dw.at[xc], 5, sib)
 
     for name in ("attn_gain", "router", "routes", "mix", "ffn_gain"):
@@ -386,7 +377,7 @@
     share_mask = iota((TC, 3 * SC), 0) // T == lax.rem(iota((TC, 3 * SC), 1), SC) // CAP
     fact_lane = iota((TC, 128), 1)
     mix_lanes = (fact_lane == 6 * experts) | (fact_lane == 6 * experts + 1)
-    F = 2 * wg.shape[1]
+    F = C * we.shape[2]
     mixing = {}
 
     def arrived_line(buf, g, k):
@@ -421,10 +412,10 @@
             ],
             axis=1,
         )
-        gate_pre = nt(received, wg[...].reshape(F, D))
-        up_pre = nt(received, wu[...].reshape(F, D))
+        gate_pre = nt(received, we[:, 0].reshape(F, D))
+        up_pre = nt(received, we[:, 1].reshape(F, D))
         hidden = (gate_pre / (1.0 + jnp.exp(-gate_pre)) * up_pre).astype(BF16)
-        partial = nn(hidden, wd[...].reshape(F, D))
+        partial = nn(hidden, we[:, 2].reshape(F, D))
         for i in range(X):
             for j in range(Y):
                 pb[g, j * X + i] = partial[
@@ -432,7 +423,7 @@
                 ].astype(BF16)
         for i, j in plane:
             px, py = plane_peer(i, j)
-            send(pb.at[g, py * X + px], pr.at[g, seat], 14 + g, (z, px, c, py))
+            send(pb.at[g, py * X + px], pr.at[g, seat], 2 + g, (z, px, c, py))
         pr[g, seat] = pb[g, seat]
 
     def stacked(a, b):
@@ -460,7 +451,7 @@
 
     def home(g):
         first = g * ZC
-        arrived(pr.at[g, pl.ds(0, X * Y - 1)], 14 + g)
+        arrived(pr.at[g, pl.ds(0, X * Y - 1)], 2 + g)
         served = jnp.zeros((SC, DY), F32)
         for k in range(X * Y):
             served = served + pr[g, k].astype(F32)
@@ -493,9 +484,7 @@
         gather(1)
 
     spread_tokens(0)
-    arrived(wg.at[0], 1)
-    arrived(wu.at[0], 2)
-    arrived(wd.at[0], 3)
+    arrived(we.at[0], 1)
     expert(0)
 
     @pl.when(early)
@@ -538,16 +527,14 @@
     out_ref[...] = ((combined - mean) * lax.rsqrt(var + 1e-05) * ffn_gain).astype(BF16)
 
     left_here(att.at[pl.ds(0, Y - 1)], 0)
-    left_here(wg.at[0], 1)
-    left_here(wu.at[0], 2)
-    left_here(wd.at[0], 3)
+    left_here(we.at[0], 1)
     left_here(dw.at[pl.ds(0, X - 1)], 4)
     left_here(dw.at[pl.ds(0, X)], 5)
     left_here(rows.at[y, pl.ds(0, Z - 1)], 8 + z // ZC)
     for g in range(CHUNKS):
         left_here(xe.at[g, pl.ds(0, X * Y - 1)], 10 + g)
         left_here(rows.at[pl.ds(0, Y - 1), pl.ds(g * ZC, ZC), :, pl.ds(0, DY)], 12 + g)
-        left_here(pb.at[g, pl.ds(0, X * Y - 1)], 14 + g)
+        left_here(pb.at[g, pl.ds(0, X * Y - 1)], 2 + g)
     left_here(fb.at[pl.ds(0, Z - 1)], 6)
     left_here(stats.at[pl.ds(0, Y - 1)], 7)
 
@@ -609,9 +596,7 @@
             V((2, HD2 // 2, D), BF16),
             V((HD2, D), BF16),
             V((experts, D), BF16),
-            V((C, F, D), BF16),
-            V((C, F, D), BF16),
-            V((C, F, D), BF16),
+            V((C, 3, F, D), BF16),
             V((FD, D), BF16),
             V((FD, D), BF16),
             V((FD, DY), BF16),
@@ -632,10 +617,9 @@
             V((D // 128, 128), F32),
             V((D // 128, 128), BF16),
             V((DY // 128, 128), F32),
-            pltpu.SemaphoreType.DMA((19,)),
-            pltpu.SemaphoreType.DMA((T,)),
-            pltpu.SemaphoreType.DMA((16,)),
-            pltpu.SemaphoreType.DMA((16,)),
+            pltpu.SemaphoreType.DMA((17,)),
+            pltpu.SemaphoreType.DMA((14,)),
+            pltpu.SemaphoreType.DMA((14,)),
             pltpu.SemaphoreType.REGULAR((dims[0],)),
             pltpu.SemaphoreType.REGULAR,
             pltpu.SemaphoreType.REGULAR,

time: 48.5 us -> 48.3 us (level)
  no operation moved by 1% of the time
where the time goes in v6:
time: 48.3 us; the launch traced here: 47.8 us
  Pallas kernels  47.2 us (98%)
  between operations  0.65 us (1%)
    pallas_call x1, Pallas kernels, body(): pl.pallas_call(functools.partial(layer_kernel, dims), out_shape=(V((T, DY...  46.6 us

profile of v6, /device:TPU:6, one launch (start us, length us, event | category | flops | bytes accessed | tf_op | source)
XLA Modules:
  0.0 47.8 jit_solution(10570325412345602795)
XLA Ops:
  0.6 46.6 %layer.1 = (bf16[8,256]{1,0:T(8,128)(2,1)S(1)}, bf16[8,128]{1,0:T(8,128)(2,1)S(1)}) custom-call(bf16[8,1024]{1,0:T(8,128)(2,1)} %tokens_hbm.1, bf16[8,1024,128]{2,1,0:T(8,128)(2,1)} %bitcast.14, s32[8]{0:T(128)} %lengths_hbm.1, bf16[1024,128]{1,0:T(8,128)(2,1)} %wq_hbm.1, bf16[64,1024]{1,0:T(8,128)(2,1)} %bitcast.17, bf16[64,1024]{1,0:T(8,128)(2,1)} %bitcast.18, ...), custom_call_target="tpu_custom_call" | custom-call | tf_op jit(solution)/shard_map/layer/pallas_call | solution.py:587
  47.2 0.6 %hand_over.1 = (bf16[8,256]{1,0:T(8,128)(2,1)}, bf16[8,128]{1,0:T(8,128)(2,1)}) custom-call(bf16[8,256]{1,0:T(8,128)(2,1)S(1)} %get-tuple-element.6.result_in, bf16[8,128]{1,0:T(8,128)(2,1)S(1)} %get-tuple-element.7.kv_in), custom_call_target="tpu_custom_call" | custom-call | tf_op jit(solution)/shard_map/hand_over/pallas_call | solution.py:655
